TPU v7x, 32 devices: a whole 2x2x4 slice. The times are simulated.
32 devices in a mesh: grp: 2 (over y), ep: 8 (over z, x), tp: 2 (over core).
Axes of the slice: x: 2, y: 2, z: 4, core: 2. Of those that a mesh axis runs over, the one named last changes fastest.
Arguments:
- tokens: bfloat16 [384, 2048], P(('grp', 'ep')), parts along dimension 0, may hold values from -6 to 6
- norm_gain: float32 [2048], replicated, may hold values from 0.1 to 1.9
- routes: int32 [384, 4], P(('grp', 'ep')), parts along dimension 0, may hold values from 0 to 7, all different within a row; in each aligned block of 24 rows (0 to 23, 24 to 47, ...) at most 24 rows name the same one
- gate_scores: float32 [384, 4], P(('grp', 'ep')), parts along dimension 0, may hold values from 0.05 to 1
- w_gate: bfloat16 [8, 2048, 512], P('ep', None, 'tp'), may hold values from -1 to 1
- w_up: bfloat16 [8, 2048, 512], P('ep', None, 'tp'), may hold values from -1 to 1
- w_down: bfloat16 [8, 512, 2048], P('ep', 'tp'), may hold values from -0.0625 to 0.0625
Outputs:
- mixed: bfloat16 [384, 2048], P(('grp', 'ep')), parts along dimension 0
There are 2 independent parts, one for each index of `grp`. A program takes and returns all parts, laid end to end along the dimension named above; an argument that names none is the same for every part. Nothing has to cross between parts.
Inputs may be any that keep to these rules, and one draw needn't show every extreme that they name: `routes`: each row names 4 different experts; among the 24 rows of one device no expert is named more than 24 times, a bound that some block reaches.
All inputs are finite; a program needn't handle non-finite values.
Results may differ from a plain program's by a relative error of at most 0.0077.
Values may be sent and summed in bfloat16 or wider, within the bound.
No kernel may reach another device: no remote copies, remote signals or barrier semaphores. Data moves between devices by JAX's collectives and lax.ppermute only.
A program may use at most 64 MiB of HBM per device.

v0:
```python
import jax
import jax.numpy as jnp
from jax import lax
from jax.sharding import PartitionSpec as P


def clamped_unit(g, u):
    gate = jnp.minimum(g, 7.0)
    up = jnp.clip(u, -7.0, 7.0)
    return (up + 1.0) * gate * jax.nn.sigmoid(1.702 * gate)


def expert_rows(rows, wg, wu, wd):
    g = jnp.dot(rows, wg, preferred_element_type=jnp.float32)
    u = jnp.dot(rows, wu, preferred_element_type=jnp.float32)
    act = clamped_unit(g, u).astype(jnp.bfloat16)
    part = jnp.dot(act, wd, preferred_element_type=jnp.float32)
    part = lax.optimization_barrier(part.astype(jnp.bfloat16)).astype(jnp.float32)
    total = lax.psum(part.astype(jnp.bfloat16), "tp")
    return total


def finish(mixed):
    result = mixed.astype(jnp.bfloat16)
    return result


def slot_table(routes, scores, experts, capacity):
    count = routes.shape[0]
    chosen = routes[:, :, None] == experts[None, None, :]
    hit = jnp.any(chosen, axis=1).astype(jnp.int32)
    weight = jnp.sum(jnp.where(chosen, scores[:, :, None], 0.0), axis=1)
    rank = jnp.cumsum(hit, axis=0) - hit
    places = jnp.arange(capacity, dtype=jnp.int32)
    match = (hit[:, :, None] == 1) & (rank[:, :, None] == places[None, None, :])
    row_ids = jnp.arange(count, dtype=jnp.int32)[:, None, None]
    filled = jnp.any(match, axis=0)
    slot_tok = jnp.sum(jnp.where(match, row_ids, 0), axis=0) + count * (
        1 - filled.astype(jnp.int32)
    )
    slot_w = jnp.sum(jnp.where(match, weight[:, :, None], 0.0), axis=0)
    return (slot_tok, slot_w)


def body(tokens, norm_gain, routes, gate_scores, w_gate, w_up, w_down):
    count, width = tokens.shape
    top = routes.shape[1]
    nexp = lax.axis_size("ep")
    capacity = max(2, min(count, 2 * count * top // nexp))
    wg, wu, wd = (w_gate[0], w_up[0], w_down[0])
    xf = tokens.astype(jnp.float32)
    normed = (xf * lax.rsqrt(jnp.mean(xf * xf, axis=-1, keepdims=True) + 1e-06) * norm_gain).astype(
        jnp.bfloat16
    )
    experts = jnp.arange(nexp, dtype=jnp.int32)
    slot_tok, slot_w = slot_table(routes, gate_scores, experts, capacity)
    padded = jnp.concatenate([normed, jnp.zeros((1, width), jnp.bfloat16)], axis=0)
    outgoing = padded[slot_tok]
    received = lax.all_to_all(outgoing, "ep", split_axis=0, concat_axis=0, tiled=True)
    sources, places, _ = received.shape
    outputs = expert_rows(received.reshape(sources * places, width), wg, wu, wd)
    returned = lax.all_to_all(
        outputs.reshape(sources, places, outputs.shape[1]),
        "ep",
        split_axis=0,
        concat_axis=0,
        tiled=True,
    )
    flat_tok = slot_tok.reshape(-1)
    token_ids = jnp.arange(count, dtype=jnp.int32)
    combine = jnp.where(flat_tok[None, :] == token_ids[:, None], slot_w.reshape(-1)[None, :], 0.0)
    mixed = jnp.dot(
        combine,
        returned.reshape(-1, returned.shape[2]).astype(jnp.float32),
        precision=lax.Precision.HIGHEST,
    )
    return finish(mixed)


def solution(mesh):
    in_specs = (
        P(("grp", "ep"), None),
        P(),
        P(("grp", "ep"), None),
        P(("grp", "ep"), None),
        P("ep", None, "tp"),
        P("ep", None, "tp"),
        P("ep", "tp", None),
    )
    out_specs = P(("grp", "ep"), None)
    return jax.shard_map(body, mesh=mesh, in_specs=in_specs, out_specs=out_specs, check_vma=False)
```

profile of v0, /device:TPU:0, one launch (start us, length us, event | category | flops | bytes accessed | tf_op | source)
XLA Modules:
  0.0 94.1 jit_solution(17916535765891462060)
XLA Ops:
  6.5 0.0 copy-start
  6.5 0.0 all-reduce.3.cloned.1.call-start
  6.5 0.8 fusion.23
  7.3 0.1 copy.10
  7.5 0.1 fusion.21
  7.6 0.1 select_reduce_fusion.1
  7.7 1.0 %fusion.8 = f32[24]{0:T(128)S(1)} fusion(bf16[24,2048]{1,0:T(8,128)(2,1)} %param.7), kind=kLoop, calls=%fused_computation.14 | loop fusion | flops 147432 | bytes 98400 | tf_op jit(solution)/shard_map/reduce_sum | solution.py:52
  8.8 0.1 reshape.96
  8.9 1.0 %fusion.10 = bf16[24,2048]{1,0:T(8,128)(2,1)S(1)} fusion(bf16[24,2048]{1,0:T(8,128)(2,1)} %param.7, f32[2048]{0:T(1024)} %param.8, f32[24]{0:T(128)S(1)} %add_rsqrt_fusion), kind=kLoop, calls=%fused_computation.16 | loop fusion | flops 196608 | bytes 204896 | tf_op jit(solution)/shard_map/convert_element_type | solution.py:52
  9.9 1.1 %gather_fusion = bf16[192,2048]{1,0:T(8,128)(2,1)S(1)} fusion(bf16[25,2048]{1,0:T(8,128)(2,1)S(1)} %concatenate.3, s32[1024]{0:T(1024)S(1)} %pad_clamp_fusion), kind=kCustom, calls=%fused_computation | custom fusion | bytes 1573632 | tf_op jit(solution)/shard_map/gather | solution.py:58
  11.0 0.0 copy-start.1
  11.0 27.4 %all_to_all.10 = bf16[8,24,2048]{2,1,0:T(8,128)(2,1)S(1)} all-to-all(bf16[8,24,2048]{2,1,0:T(8,128)(2,1)S(1)} %bitcast.23), channel_id=1, replica_groups=mesh['grp'=2,'ep'=8,'tp'=2] {'ep'}, dimensions={0} | all-to-all | bytes 1572864 | tf_op jit(solution)/shard_map/all_to_all | solution.py:59
  38.4 0.0 copy-start.2
  38.4 0.0 copy-done.1
  38.4 0.4 convolution_minimum_fusion
  38.8 0.0 copy-done
  38.8 0.8 copy-done.2
  39.6 1.9 %convolution_convert_fusion = bf16[192,2048]{1,0:T(8,128)(2,1)} fusion(f32[192,256]{1,0:T(8,128)S(1)} %convolution_minimum_fusion, bf16[192,2048]{1,0:T(8,128)(2,1)S(1)} %bitcast.22, bf16[1,256,2048]{2,1,0:T(8,128)(2,1)S(1)} %copy-done, bf16[1,2048,256]{2,1,0:T(8,128)(2,1)S(1)} %copy-done.2), kind=kOutput, calls=%fused_computation.1 | convolution fusion | flops 403488768 | bytes 3866624 | tf_op jit(solution)/shard_map/dot_general | solution.py:17
  41.6 0.0 copy-start.3
  41.6 0.0 copy-start.4
  41.6 0.0 all-reduce.3.cloned.1.call-update
  41.6 18.2 %all-reduce.3.cloned.1.call-done = bf16[8,24,2048]{2,1,0:T(8,128)(2,1)} async-done(((bf16[8,24,2048]{2,1,0:T(8,128)(2,1)}), bf16[8,24,2048]{2,1,0:T(8,128)(2,1)}) %all-reduce.3.cloned.1.call-update) | async-done | bytes 786448 | tf_op jit(solution)/shard_map/psum | solution.py:19
  59.8 5.8 %all-to-all-start.1 = ((bf16[8,24,2048]{2,1,0:T(8,128)(2,1)}), bf16[8,24,2048]{2,1,0:T(8,128)(2,1)S(1)}, u32[]{:S(2)}, u32[]{:S(2)}) async-start(bf16[8,24,2048]{2,1,0:T(8,128)(2,1)} %all-reduce.3.cloned.1.call-done), calls=%async_computation.1 | async-start | bytes 1572864 | tf_op jit(solution)/shard_map/all_to_all | solution.py:62
  65.6 0.0 copy-done.3
  65.6 0.0 copy-done.4
  65.6 0.1 copy.11
  65.7 0.1 select_reduce_fusion
  65.8 0.1 broadcast_in_dim.69
  65.9 0.1 add.52
  66.0 20.2 %all-to-all-done.1 = bf16[8,24,2048]{2,1,0:T(8,128)(2,1)S(1)} async-done(((bf16[8,24,2048]{2,1,0:T(8,128)(2,1)}), bf16[8,24,2048]{2,1,0:T(8,128)(2,1)S(1)}, u32[]{:S(2)}, u32[]{:S(2)}) %all-to-all-start.1) | async-done | bytes 786464 | tf_op jit(solution)/shard_map/all_to_all | solution.py:62
  86.1 1.1 %convolution_convert_fusion.1 = bf16[24,2048]{1,0:T(8,128)(2,1)} fusion(bf16[192,2048]{1,0:T(8,128)(2,1)S(1)} %bitcast.24, f32[192]{0:T(256)S(1)} %broadcast_in_dim.69, s32[192]{0:T(256)S(1)} %add.52), kind=kOutput, calls=%fused_computation.2 | convolution fusion | flops 113304576 | bytes 886272 | tf_op jit(solution)/shard_map/dot_general | solution.py:72
  (8 shorter events, 0.1 us)
Async XLA Ops:
  6.5 32.3 %copy-start = (bf16[1,256,2048]{2,1,0:T(8,128)(2,1)S(1)}, bf16[1,256,2048]{2,1,0:T(8,128)(2,1)}, u32[]{:S(2)}) copy-start(bf16[1,256,2048]{2,1,0:T(8,128)(2,1)} %param.13) | copy-start | bytes 3145732
  6.5 53.2 %all-reduce.3.cloned.1.call-start = ((), (), s32[]{:S(2)}) async-start(), calls=%async_computation.2 | async-start | bytes 1572864 | tf_op jit(solution)/shard_map/psum | solution.py:19
  11.0 27.4 %copy-start.1 = (bf16[1,2048,256]{2,1,0:T(8,128)(2,1)S(1)}, bf16[1,2048,256]{2,1,0:T(8,128)(2,1)}, u32[]{:S(2)}) copy-start(bf16[1,2048,256]{2,1,0:T(8,128)(2,1)} %param.11) | copy-start | bytes 3145732
  38.4 1.2 %copy-start.2 = (bf16[1,2048,256]{2,1,0:T(8,128)(2,1)S(1)}, bf16[1,2048,256]{2,1,0:T(8,128)(2,1)}, u32[]{:S(2)}) copy-start(bf16[1,2048,256]{2,1,0:T(8,128)(2,1)} %param.12) | copy-start | bytes 3145732
  41.6 24.0 %copy-start.3 = (s32[24,4]{0,1:T(4,128)S(1)}, s32[24,4]{0,1:T(4,128)}, u32[]{:S(2)}) copy-start(s32[24,4]{0,1:T(4,128)} %param.9) | copy-start | bytes 1156
  41.6 24.0 %copy-start.4 = (f32[24,4]{0,1:T(4,128)S(1)}, f32[24,4]{0,1:T(4,128)}, u32[]{:S(2)}) copy-start(f32[24,4]{0,1:T(4,128)} %param.10) | copy-start | bytes 1156
  59.8 26.4 %all-to-all-start.1 = ((bf16[8,24,2048]{2,1,0:T(8,128)(2,1)}), bf16[8,24,2048]{2,1,0:T(8,128)(2,1)S(1)}, u32[]{:S(2)}, u32[]{:S(2)}) async-start(bf16[8,24,2048]{2,1,0:T(8,128)(2,1)} %all-reduce.3.cloned.1.call-done), calls=%async_computation.1 | async-start | bytes 1572864 | tf_op jit(solution)/shard_map/all_to_all | solution.py:62
Sparse Core Ops, SparseCore 0:
  41.7 17.9 all-reduce.2
where the time goes:
time: 94.4 us; the launch traced here: 94.1 us
  waiting for transfers between devices  38.3 us (41%)
  blocking collectives  27.4 us (29%)
  between operations  13.5 us (14%)
  starting transfers between devices  5.81 us (6%)
  matrix products  3.4 us (4%)
  other arithmetic  3.26 us (3%)
  local copies, waits for them, and re-layouts  2.39 us (3%)
    all_to_all x1, blocking collectives, body(): lax.all_to_all(outgoing, 'ep', split_axis=0, concat_axis=0, tiled=True)  27.4 us
    all_to_all x1, waiting for transfers between devices, body(): lax.all_to_all(outputs.reshape(sources, places, outputs.shape[1]), 'ep',...  20.2 us
    psum x1, waiting for transfers between devices, expert_rows(): total = lax.psum(part.astype(jnp.bfloat16), 'tp')  18.2 us
    all_to_all x1, starting transfers between devices, body(): lax.all_to_all(outputs.reshape(sources, places, outputs.shape[1]), 'ep',...  5.81 us
    dot_general x1, matrix products, expert_rows(): part = jnp.dot(act, wd, preferred_element_type=jnp.float32)  1.94 us
  transfers between devices with their start and end apart: 2, of which 2 were waited for; matrix products, arithmetic and copies ran while one was open for 0% of the time, Pallas kernels for 0%

commit v1 on v0

--- a/solution.py
+++ b/solution.py
@@ -25,6 +25,12 @@
     return result
 
 
+def normalise(tokens, norm_gain):
+    xf = tokens.astype(jnp.float32)
+    scale = lax.rsqrt(jnp.mean(xf * xf, axis=-1, keepdims=True) + 1e-06)
+    return (xf * scale * norm_gain).astype(jnp.bfloat16)
+
+
 def slot_table(routes, scores, experts, capacity):
     count = routes.shape[0]
     chosen = routes[:, :, None] == experts[None, None, :]
@@ -42,16 +48,11 @@
     return (slot_tok, slot_w)
 
 
-def body(tokens, norm_gain, routes, gate_scores, w_gate, w_up, w_down):
+def slotted(tokens, norm_gain, routes, gate_scores, w_gate, w_up, w_down, capacity):
     count, width = tokens.shape
-    top = routes.shape[1]
     nexp = lax.axis_size("ep")
-    capacity = max(2, min(count, 2 * count * top // nexp))
     wg, wu, wd = (w_gate[0], w_up[0], w_down[0])
-    xf = tokens.astype(jnp.float32)
-    normed = (xf * lax.rsqrt(jnp.mean(xf * xf, axis=-1, keepdims=True) + 1e-06) * norm_gain).astype(
-        jnp.bfloat16
-    )
+    normed = normalise(tokens, norm_gain)
     experts = jnp.arange(nexp, dtype=jnp.int32)
     slot_tok, slot_w = slot_table(routes, gate_scores, experts, capacity)
     padded = jnp.concatenate([normed, jnp.zeros((1, width), jnp.bfloat16)], axis=0)
@@ -77,6 +78,71 @@
     return finish(mixed)
 
 
+def swap(x, axis, mask):
+    size = lax.axis_size(axis)
+    return lax.ppermute(x, axis, [(i, i ^ mask) for i in range(size)])
+
+
+def dense(tokens, norm_gain, routes, gate_scores, w_gate, w_up, w_down):
+    count, width = tokens.shape
+    nexp = lax.axis_size("ep")
+    half = width // 2
+    tp = lax.axis_index("tp")
+    wg, wu, wd = (w_gate[0], w_up[0], w_down[0])
+    masks = [1 << b for b in reversed(range((nexp - 1).bit_length()))]
+
+    lanes = -(-nexp // 128) * 128
+    experts = jnp.arange(lanes, dtype=jnp.int32)
+    chosen = routes[:, :, None] == experts[None, None, :]
+    weight = jnp.sum(jnp.where(chosen, gate_scores[:, :, None], 0.0), axis=1)
+    high = weight.astype(jnp.bfloat16)
+    low = (weight - lax.reduce_precision(weight, 8, 7)).astype(jnp.bfloat16)
+
+    xf = tokens.astype(jnp.float32)
+    scale = lax.rsqrt(jnp.mean(xf * xf, axis=-1, keepdims=True) + 1e-06)
+    own_x = lax.dynamic_slice_in_dim(xf, tp * half, half, 1)
+    own_gain = lax.dynamic_slice_in_dim(norm_gain, tp * half, half, 0)
+    normed = (own_x * scale * own_gain).astype(jnp.bfloat16)
+    rows = jnp.concatenate([normed, jnp.where(tp == 0, high, low)], axis=1)
+    for mask in masks:
+        rows = jnp.concatenate([rows, swap(rows, "ep", mask)], axis=0)
+    both = lax.all_gather(rows, "tp")
+    full = jnp.concatenate([both[0, :, :half], both[1, :, :half]], axis=1)
+    pair = both[0, :, half:].astype(jnp.float32) + both[1, :, half:].astype(jnp.float32)
+    mine = (experts == lax.axis_index("ep"))[None, :]
+    score = jnp.sum(jnp.where(mine, pair, 0.0), axis=1, keepdims=True)
+
+    g = jnp.dot(full, wg, preferred_element_type=jnp.float32)
+    u = jnp.dot(full, wu, preferred_element_type=jnp.float32)
+    act = clamped_unit(g, u).astype(jnp.bfloat16)
+    wd_own = lax.dynamic_slice_in_dim(wd, tp * half, half, 1)
+    wd_other = lax.dynamic_slice_in_dim(wd, (1 - tp) * half, half, 1)
+    other = jnp.dot(act, wd_other, preferred_element_type=jnp.float32).astype(jnp.bfloat16)
+    other = swap(other, "tp", 1)
+    own = jnp.dot(act, wd_own, preferred_element_type=jnp.float32)
+    total = (own + other.astype(jnp.float32)) * score
+    for mask in reversed(masks):
+        n = total.shape[0] // 2
+        sent = swap(total[n:].astype(jnp.bfloat16), "ep", mask)
+        total = total[:n] + sent.astype(jnp.float32)
+    mixed = finish(total)
+    theirs = swap(mixed, "tp", 1)
+    return jnp.concatenate(
+        [jnp.where(tp == 0, mixed, theirs), jnp.where(tp == 0, theirs, mixed)], axis=1
+    )
+
+
+def body(tokens, norm_gain, routes, gate_scores, w_gate, w_up, w_down):
+    args = (tokens, norm_gain, routes, gate_scores, w_gate, w_up, w_down)
+    count = tokens.shape[0]
+    top = routes.shape[1]
+    nexp = lax.axis_size("ep")
+    capacity = max(2, min(count, 2 * count * top // nexp))
+    if capacity == count and nexp & (nexp - 1) == 0 and lax.axis_size("tp") == 2:
+        return dense(*args)
+    return slotted(*args, capacity)
+
+
 def solution(mesh):
     in_specs = (
         P(("grp", "ep"), None),

time: 94.4 us -> 48.2 us (0.51)
  blocking collectives: 27.4 us -> 2.44 us
  waiting for transfers between devices: 38.3 us -> 24.2 us
  between operations: 13.5 us -> 0.16 us
  starting transfers between devices: 5.81 us -> 13.2 us
  matrix products: 3.4 us -> 1.3 us
    all_to_all x1 -> x0, blocking collectives: 27.4 us -> none  [body(): lax.all_to_all(outgoing, 'ep', split_axis=0, concat_axis=0, tiled=True)]
    ppermute x0 -> x8, waiting for transfers between devices: none -> 24.2 us  [swap(): return lax.ppermute(x, axis, [(i, i ^ mask) for i in range(size)])]
    all_to_all x1 -> x0, waiting for transfers between devices: 20.2 us -> none  [body(): lax.all_to_all(outputs.reshape(sources, places, outputs.shape[1]), 'ep',...]
    psum x1 -> x0, waiting for transfers between devices: 18.2 us -> none  [expert_rows(): total = lax.psum(part.astype(jnp.bfloat16), 'tp')]
    ppermute x0 -> x8, starting transfers between devices: none -> 13.2 us  [swap(): return lax.ppermute(x, axis, [(i, i ^ mask) for i in range(size)])]
    all_to_all x1 -> x0, starting transfers between devices: 5.81 us -> none  [body(): lax.all_to_all(outputs.reshape(sources, places, outputs.shape[1]), 'ep',...]
    all_gather x0 -> x1, blocking collectives: none -> 2.44 us  [dense(): both = lax.all_gather(rows, 'tp')]
    dot_general x3 -> x4, matrix products: 3.4 us -> 1.3 us  [the longest x1 0.38 us: dense(): u = jnp.dot(full, wu, preferred_element_type=jnp.float32)]
  transfers between devices with their start and end apart: 2 -> 8, of which waited for: 2 -> 8; matrix products, arithmetic and copies ran while one was open for 0% -> 0% of each run, Pallas kernels for 0% -> 0%
where the time goes in v1:
time: 48.2 us; the launch traced here: 47.9 us
  waiting for transfers between devices  24.2 us (50%)
  starting transfers between devices  13.2 us (27%)
  other arithmetic  3.84 us (8%)
  local copies, waits for them, and re-layouts  2.8 us (6%)
  blocking collectives  2.44 us (5%)
  matrix products  1.3 us (3%)
    ppermute x8, waiting for transfers between devices, swap(): return lax.ppermute(x, axis, [(i, i ^ mask) for i in range(size)])  24.2 us
    ppermute x8, starting transfers between devices, swap(): return lax.ppermute(x, axis, [(i, i ^ mask) for i in range(size)])  13.2 us
    all_gather x1, blocking collectives, dense(): both = lax.all_gather(rows, 'tp')  2.44 us
    unnamed x6, local copies, waits for them, and re-layouts  1.97 us
    reduce_sum x1, other arithmetic, dense(): scale = lax.rsqrt(jnp.mean(xf * xf, axis=-1, keepdims=True) + 1e-06)  1.11 us
  transfers between devices with their start and end apart: 8, of which 8 were waited for; matrix products, arithmetic and copies ran while one was open for 0% of the time, Pallas kernels for 0%

profile of v1, /device:TPU:0, one launch (start us, length us, event | category | flops | bytes accessed | tf_op | source)
XLA Modules:
  0.0 47.9 jit_solution(9930509602255946921)
XLA Ops:
  0.0 0.0 copy-start
  0.0 1.1 %multiply_reduce_fusion = f32[24]{0:T(128)S(1)} fusion(bf16[24,2048]{1,0:T(8,128)(2,1)} %param.7), kind=kLoop, calls=%fused_computation.24 | loop fusion | flops 147432 | bytes 98400 | tf_op jit(solution)/shard_map/reduce_sum | solution.py:102
  1.1 0.9 %convert_element_type.44 = f32[24,2048]{1,0:T(8,128)S(1)} convert(bf16[24,2048]{1,0:T(8,128)(2,1)} %param.7) | non-fusion elementwise | flops 49152 | bytes 294912 | tf_op jit(solution)/shard_map/convert_element_type | solution.py:101
  2.0 0.7 %dynamic_slice.17 = f32[1024]{0:T(1024)S(1)} dynamic-slice(f32[2048]{0:T(1024)} %param.8, s32[]{:T(128)S(6)} %select_n.37), dynamic_slice_sizes={1024} | dynamic-slice | bytes 8196 | tf_op jit(solution)/shard_map/dynamic_slice | solution.py:104
  2.7 0.8 %select_reduce_fusion = f32[24,128]{1,0:T(8,128)S(1)} fusion(f32[24,4]{0,1:T(4,128)} %param.10, s32[24,4]{0,1:T(4,128)} %param.9), kind=kLoop, calls=%fused_computation.34 | loop fusion | flops 33792 | bytes 13056 | tf_op jit(solution)/shard_map/reduce_sum | solution.py:97
  3.5 0.1 multiply_convert_fusion
  3.7 4.1 %collective-permute-start = (bf16[24,1152]{1,0:T(8,128)(2,1)S(1)}, bf16[24,1152]{1,0:T(8,128)(2,1)S(1)}, u32[]{:S(2)}, u32[]{:S(2)}) collective-permute-start(bf16[24,1152]{1,0:T(8,128)(2,1)S(1)} %pad_maximum_fusion.7), channel_id=1, source_target_pairs={{0,8},{2,10},{4,12},{6,14},{8,0},{10,2},{12,4},{14,6},{1,9},{3,11}... | collective-permute-start | bytes 165896 | tf_op jit(solution)/shard_map/ppermute | solution.py:83
  7.8 2.7 %collective-permute-done = bf16[24,1152]{1,0:T(8,128)(2,1)S(1)} collective-permute-done((bf16[24,1152]{1,0:T(8,128)(2,1)S(1)}, bf16[24,1152]{1,0:T(8,128)(2,1)S(1)}, u32[]{:S(2)}, u32[]{:S(2)}) %collective-permute-start) | collective-permute-done | bytes 55328 | tf_op jit(solution)/shard_map/ppermute | solution.py:83
  10.5 1.4 %collective-permute-start.1 = (bf16[48,1152]{1,0:T(8,128)(2,1)S(1)}, bf16[48,1152]{1,0:T(8,128)(2,1)S(1)}, u32[]{:S(2)}, u32[]{:S(2)}) collective-permute-start(bf16[48,1152]{1,0:T(8,128)(2,1)S(1)} %pad_maximum_fusion.5), channel_id=1, source_target_pairs={{0,4},{2,6},{4,0},{6,2},{8,12},{10,14},{12,8},{14,10},{1,5},{3,7},... | collective-permute-start | bytes 331784 | tf_op jit(solution)/shard_map/ppermute | solution.py:83
  11.9 3.4 %collective-permute-done.1 = bf16[48,1152]{1,0:T(8,128)(2,1)S(1)} collective-permute-done((bf16[48,1152]{1,0:T(8,128)(2,1)S(1)}, bf16[48,1152]{1,0:T(8,128)(2,1)S(1)}, u32[]{:S(2)}, u32[]{:S(2)}) %collective-permute-start.1) | collective-permute-done | bytes 110624 | tf_op jit(solution)/shard_map/ppermute | solution.py:83
  15.4 1.8 %collective-permute-start.2 = (bf16[96,1152]{1,0:T(8,128)(2,1)S(1)}, bf16[96,1152]{1,0:T(8,128)(2,1)S(1)}, u32[]{:S(2)}, u32[]{:S(2)}) collective-permute-start(bf16[96,1152]{1,0:T(8,128)(2,1)S(1)} %pad_maximum_fusion.4), channel_id=1, source_target_pairs={{0,2},{2,0},{4,6},{6,4},{8,10},{10,8},{12,14},{14,12},{1,3},{3,1},... | collective-permute-start | bytes 663560 | tf_op jit(solution)/shard_map/ppermute | solution.py:83
  17.1 4.2 %collective-permute-done.2 = bf16[96,1152]{1,0:T(8,128)(2,1)S(1)} collective-permute-done((bf16[96,1152]{1,0:T(8,128)(2,1)S(1)}, bf16[96,1152]{1,0:T(8,128)(2,1)S(1)}, u32[]{:S(2)}, u32[]{:S(2)}) %collective-permute-start.2) | collective-permute-done | bytes 221216 | tf_op jit(solution)/shard_map/ppermute | solution.py:83
  21.4 2.4 %all-gather = bf16[384,1152]{1,0:T(8,128)(2,1)S(1)} all-gather(bf16[192,1152]{1,0:T(8,128)(2,1)S(1)} %pad_maximum_fusion.3), channel_id=2, replica_groups=mesh['grp'=2,'ep'=8,'tp'=2] {'tp'}, dimensions={0}, use_global_device_ids=true | all-gather | bytes 1327104 | tf_op jit(solution)/shard_map/all_gather | solution.py:109
  23.8 0.0 copy-start.1
  23.8 0.1 slice_bitcast_fusion.1
  23.9 1.1 %copy-done.1 = bf16[1,2048,256]{2,1,0:T(8,128)(2,1)S(1)} copy-done((bf16[1,2048,256]{2,1,0:T(8,128)(2,1)S(1)}, bf16[1,2048,256]{2,1,0:T(8,128)(2,1)}, u32[]{:S(2)}) %copy-start.1) | copy-done | bytes 1048600
  25.1 0.0 copy-start.2
  25.1 0.4 convolution_minimum_fusion
  25.5 0.8 %copy-done.2 = bf16[1,2048,256]{2,1,0:T(8,128)(2,1)S(1)} copy-done((bf16[1,2048,256]{2,1,0:T(8,128)(2,1)S(1)}, bf16[1,2048,256]{2,1,0:T(8,128)(2,1)}, u32[]{:S(2)}) %copy-start.2) | copy-done | bytes 1048600
  26.3 0.4 fusion.3
  26.7 0.0 copy-done
  26.7 0.3 convolution_convert_fusion
  27.0 0.2 collective-permute-start.3
  27.2 0.1 fusion.14
  27.3 1.5 %collective-permute-done.3 = bf16[192,1024]{1,0:T(8,128)(2,1)S(1)} collective-permute-done((bf16[192,1024]{1,0:T(8,128)(2,1)S(1)}, bf16[192,1024]{1,0:T(8,128)(2,1)S(1)}, u32[]{:S(2)}, u32[]{:S(2)}) %collective-permute-start.3) | collective-permute-done | bytes 393248 | tf_op jit(solution)/shard_map/ppermute | solution.py:83
  28.8 0.3 add_multiply_fusion
  29.1 1.8 %collective-permute-start.4 = (bf16[96,1024]{1,0:T(8,128)(2,1)S(1)}, bf16[96,1024]{1,0:T(8,128)(2,1)S(1)}, u32[]{:S(2)}, u32[]{:S(2)}) collective-permute-start(bf16[96,1024]{1,0:T(8,128)(2,1)S(1)} %slice.65), channel_id=1, source_target_pairs={{0,2},{2,0},{4,6},{6,4},{8,10},{10,8},{12,14},{14,12},{1,3},{3,1},... | collective-permute-start | bytes 589832 | tf_op jit(solution)/shard_map/ppermute | solution.py:83
  30.9 5.2 %collective-permute-done.4 = bf16[96,1024]{1,0:T(8,128)(2,1)S(1)} collective-permute-done((bf16[96,1024]{1,0:T(8,128)(2,1)S(1)}, bf16[96,1024]{1,0:T(8,128)(2,1)S(1)}, u32[]{:S(2)}, u32[]{:S(2)}) %collective-permute-start.4) | collective-permute-done | bytes 196640 | tf_op jit(solution)/shard_map/ppermute | solution.py:83
  36.2 1.4 %collective-permute-start.5 = (bf16[48,1024]{1,0:T(8,128)(2,1)S(1)}, bf16[48,1024]{1,0:T(8,128)(2,1)S(1)}, u32[]{:S(2)}, u32[]{:S(2)}) collective-permute-start(bf16[48,1024]{1,0:T(8,128)(2,1)S(1)} %slice.66), channel_id=1, source_target_pairs={{0,4},{2,6},{4,0},{6,2},{8,12},{10,14},{12,8},{14,10},{1,5},{3,7},... | collective-permute-start | bytes 294920 | tf_op jit(solution)/shard_map/ppermute | solution.py:83
  37.5 3.3 %collective-permute-done.5 = bf16[48,1024]{1,0:T(8,128)(2,1)S(1)} collective-permute-done((bf16[48,1024]{1,0:T(8,128)(2,1)S(1)}, bf16[48,1024]{1,0:T(8,128)(2,1)S(1)}, u32[]{:S(2)}, u32[]{:S(2)}) %collective-permute-start.5) | collective-permute-done | bytes 98336 | tf_op jit(solution)/shard_map/ppermute | solution.py:83
  40.9 2.5 %collective-permute-start.6 = (bf16[24,1024]{1,0:T(8,128)(2,1)S(1)}, bf16[24,1024]{1,0:T(8,128)(2,1)S(1)}, u32[]{:S(2)}, u32[]{:S(2)}) collective-permute-start(bf16[24,1024]{1,0:T(8,128)(2,1)S(1)} %slice.67), channel_id=1, source_target_pairs={{0,8},{2,10},{4,12},{6,14},{8,0},{10,2},{12,4},{14,6},{1,9},{3,11}... | collective-permute-start | bytes 147464 | tf_op jit(solution)/shard_map/ppermute | solution.py:83
  43.4 2.6 %collective-permute-done.6 = bf16[24,1024]{1,0:T(8,128)(2,1)S(1)} collective-permute-done((bf16[24,1024]{1,0:T(8,128)(2,1)S(1)}, bf16[24,1024]{1,0:T(8,128)(2,1)S(1)}, u32[]{:S(2)}, u32[]{:S(2)}) %collective-permute-start.6) | collective-permute-done | bytes 49184 | tf_op jit(solution)/shard_map/ppermute | solution.py:83
  45.9 0.1 collective-permute-start.7
  46.0 1.2 %collective-permute-done.7 = bf16[24,1024]{1,0:T(8,128)(2,1)S(1)} collective-permute-done((bf16[24,1024]{1,0:T(8,128)(2,1)S(1)}, bf16[24,1024]{1,0:T(8,128)(2,1)S(1)}, u32[]{:S(2)}, u32[]{:S(2)}) %collective-permute-start.7) | collective-permute-done | bytes 49184 | tf_op jit(solution)/shard_map/ppermute | solution.py:83
  47.3 0.6 %pad_maximum_fusion.6 = bf16[24,2048]{1,0:T(8,128)(2,1)} fusion(bf16[24,1024]{1,0:T(8,128)(2,1)S(1)} %get-tuple-element.8, bf16[24,1024]{1,0:T(8,128)(2,1)S(1)} %get-tuple-element.7), kind=kLoop, calls=%fused_computation.29 | loop fusion | flops 196608 | bytes 196608 | tf_op jit(solution)/shard_map/concatenate | solution.py:130
  (14 shorter events, 0.2 us)
Async XLA Ops:
  0.0 26.7 %copy-start = (bf16[1,256,2048]{2,1,0:T(8,128)(2,1)S(1)}, bf16[1,256,2048]{2,1,0:T(8,128)(2,1)}, u32[]{:S(2)}) copy-start(bf16[1,256,2048]{2,1,0:T(8,128)(2,1)} %param.13) | copy-start | bytes 3145732
  3.7 6.9 %collective-permute-start = (bf16[24,1152]{1,0:T(8,128)(2,1)S(1)}, bf16[24,1152]{1,0:T(8,128)(2,1)S(1)}, u32[]{:S(2)}, u32[]{:S(2)}) collective-permute-start(bf16[24,1152]{1,0:T(8,128)(2,1)S(1)} %pad_maximum_fusion.7), channel_id=1, source_target_pairs={{0,8},{2,10},{4,12},{6,14},{8,0},{10,2},{12,4},{14,6},{1,9},{3,11}... | collective-permute-start | bytes 165896 | tf_op jit(solution)/shard_map/ppermute | solution.py:83
  10.5 4.8 %collective-permute-start.1 = (bf16[48,1152]{1,0:T(8,128)(2,1)S(1)}, bf16[48,1152]{1,0:T(8,128)(2,1)S(1)}, u32[]{:S(2)}, u32[]{:S(2)}) collective-permute-start(bf16[48,1152]{1,0:T(8,128)(2,1)S(1)} %pad_maximum_fusion.5), channel_id=1, source_target_pairs={{0,4},{2,6},{4,0},{6,2},{8,12},{10,14},{12,8},{14,10},{1,5},{3,7},... | collective-permute-start | bytes 331784 | tf_op jit(solution)/shard_map/ppermute | solution.py:83
  15.4 6.0 %collective-permute-start.2 = (bf16[96,1152]{1,0:T(8,128)(2,1)S(1)}, bf16[96,1152]{1,0:T(8,128)(2,1)S(1)}, u32[]{:S(2)}, u32[]{:S(2)}) collective-permute-start(bf16[96,1152]{1,0:T(8,128)(2,1)S(1)} %pad_maximum_fusion.4), channel_id=1, source_target_pairs={{0,2},{2,0},{4,6},{6,4},{8,10},{10,8},{12,14},{14,12},{1,3},{3,1},... | collective-permute-start | bytes 663560 | tf_op jit(solution)/shard_map/ppermute | solution.py:83
  23.8 1.2 %copy-start.1 = (bf16[1,2048,256]{2,1,0:T(8,128)(2,1)S(1)}, bf16[1,2048,256]{2,1,0:T(8,128)(2,1)}, u32[]{:S(2)}) copy-start(bf16[1,2048,256]{2,1,0:T(8,128)(2,1)} %param.11) | copy-start | bytes 3145732
  25.1 1.2 %copy-start.2 = (bf16[1,2048,256]{2,1,0:T(8,128)(2,1)S(1)}, bf16[1,2048,256]{2,1,0:T(8,128)(2,1)}, u32[]{:S(2)}) copy-start(bf16[1,2048,256]{2,1,0:T(8,128)(2,1)} %param.12) | copy-start | bytes 3145732
  27.0 1.8 %collective-permute-start.3 = (bf16[192,1024]{1,0:T(8,128)(2,1)S(1)}, bf16[192,1024]{1,0:T(8,128)(2,1)S(1)}, u32[]{:S(2)}, u32[]{:S(2)}) collective-permute-start(bf16[192,1024]{1,0:T(8,128)(2,1)S(1)} %convolution_convert_fusion), channel_id=1, source_target_pairs={{0,1},{1,0},{2,3},{3,2},{4,5},{5,4},{6,7},{7,6},{8,9},{9,8},{10,11... | collective-permute-start | bytes 1179656 | tf_op jit(solution)/shard_map/ppermute | solution.py:83
  29.1 7.0 %collective-permute-start.4 = (bf16[96,1024]{1,0:T(8,128)(2,1)S(1)}, bf16[96,1024]{1,0:T(8,128)(2,1)S(1)}, u32[]{:S(2)}, u32[]{:S(2)}) collective-permute-start(bf16[96,1024]{1,0:T(8,128)(2,1)S(1)} %slice.65), channel_id=1, source_target_pairs={{0,2},{2,0},{4,6},{6,4},{8,10},{10,8},{12,14},{14,12},{1,3},{3,1},... | collective-permute-start | bytes 589832 | tf_op jit(solution)/shard_map/ppermute | solution.py:83
  36.2 4.7 %collective-permute-start.5 = (bf16[48,1024]{1,0:T(8,128)(2,1)S(1)}, bf16[48,1024]{1,0:T(8,128)(2,1)S(1)}, u32[]{:S(2)}, u32[]{:S(2)}) collective-permute-start(bf16[48,1024]{1,0:T(8,128)(2,1)S(1)} %slice.66), channel_id=1, source_target_pairs={{0,4},{2,6},{4,0},{6,2},{8,12},{10,14},{12,8},{14,10},{1,5},{3,7},... | collective-permute-start | bytes 294920 | tf_op jit(solution)/shard_map/ppermute | solution.py:83
  40.9 5.1 %collective-permute-start.6 = (bf16[24,1024]{1,0:T(8,128)(2,1)S(1)}, bf16[24,1024]{1,0:T(8,128)(2,1)S(1)}, u32[]{:S(2)}, u32[]{:S(2)}) collective-permute-start(bf16[24,1024]{1,0:T(8,128)(2,1)S(1)} %slice.67), channel_id=1, source_target_pairs={{0,8},{2,10},{4,12},{6,14},{8,0},{10,2},{12,4},{14,6},{1,9},{3,11}... | collective-permute-start | bytes 147464 | tf_op jit(solution)/shard_map/ppermute | solution.py:83
  45.9 1.3 %collective-permute-start.7 = (bf16[24,1024]{1,0:T(8,128)(2,1)S(1)}, bf16[24,1024]{1,0:T(8,128)(2,1)S(1)}, u32[]{:S(2)}, u32[]{:S(2)}) collective-permute-start(bf16[24,1024]{1,0:T(8,128)(2,1)S(1)} %fusion.13), channel_id=1, source_target_pairs={{0,1},{1,0},{2,3},{3,2},{4,5},{5,4},{6,7},{7,6},{8,9},{9,8},{10,11... | collective-permute-start | bytes 147464 | tf_op jit(solution)/shard_map/ppermute | solution.py:83

commit v2 on v0

--- a/solution.py
+++ b/solution.py
@@ -1,6 +1,7 @@
 import jax
 import jax.numpy as jnp
 from jax import lax
+from jax.experimental import pallas as pl
 from jax.sharding import PartitionSpec as P
 
 
@@ -23,6 +24,12 @@
 def finish(mixed):
     result = mixed.astype(jnp.bfloat16)
     return result
+
+
+def normalise(tokens, norm_gain):
+    xf = tokens.astype(jnp.float32)
+    scale = lax.rsqrt(jnp.mean(xf * xf, axis=-1, keepdims=True) + 1e-06)
+    return (xf * scale * norm_gain).astype(jnp.bfloat16)
 
 
 def slot_table(routes, scores, experts, capacity):
@@ -42,16 +49,11 @@
     return (slot_tok, slot_w)
 
 
-def body(tokens, norm_gain, routes, gate_scores, w_gate, w_up, w_down):
+def slotted(tokens, norm_gain, routes, gate_scores, w_gate, w_up, w_down, capacity):
     count, width = tokens.shape
-    top = routes.shape[1]
     nexp = lax.axis_size("ep")
-    capacity = max(2, min(count, 2 * count * top // nexp))
     wg, wu, wd = (w_gate[0], w_up[0], w_down[0])
-    xf = tokens.astype(jnp.float32)
-    normed = (xf * lax.rsqrt(jnp.mean(xf * xf, axis=-1, keepdims=True) + 1e-06) * norm_gain).astype(
-        jnp.bfloat16
-    )
+    normed = normalise(tokens, norm_gain)
     experts = jnp.arange(nexp, dtype=jnp.int32)
     slot_tok, slot_w = slot_table(routes, gate_scores, experts, capacity)
     padded = jnp.concatenate([normed, jnp.zeros((1, width), jnp.bfloat16)], axis=0)
@@ -77,6 +79,117 @@
     return finish(mixed)
 
 
+def swap(x, mask):
+    nexp, cores = lax.axis_size("ep"), lax.axis_size("tp")
+    if mask is None:
+        return lax.ppermute(x, "tp", [(c, c ^ 1) for c in range(cores)])
+    pairs = [(e * cores + c, (e ^ mask[c]) * cores + c) for e in range(nexp) for c in range(cores)]
+    return lax.ppermute(x, ("ep", "tp"), pairs)
+
+
+def prepare(tokens, norm_gain, routes, gate_scores, lanes):
+    count, width = tokens.shape
+    half = width // 2
+    top = routes.shape[1]
+
+    def kernel(x_ref, gain_ref, route_ref, score_ref, out_ref):
+        first = lax.axis_index("tp") == 0
+        x = x_ref[...].astype(jnp.float32)
+        scale = lax.rsqrt(jnp.mean(x * x, axis=-1, keepdims=True) + 1e-06)
+        normed = x * scale * gain_ref[...]
+        out_ref[:, :half] = jnp.where(first, normed[:, :half], normed[:, half:]).astype(jnp.bfloat16)
+        expert = lax.broadcasted_iota(jnp.int32, (lanes, count), 0)
+        weight = jnp.zeros((lanes, count), jnp.float32)
+        for k in range(top):
+            weight += jnp.where(route_ref[k : k + 1, :] == expert, score_ref[k : k + 1, :], 0.0)
+        high = weight.astype(jnp.bfloat16)
+        low = (weight - high.astype(jnp.float32)).astype(jnp.bfloat16)
+        term = jnp.where(first, high.astype(jnp.float32), low.astype(jnp.float32)).astype(jnp.bfloat16)
+        row = lax.broadcasted_iota(jnp.int32, (lanes, lanes), 0)
+        col = lax.broadcasted_iota(jnp.int32, (lanes, lanes), 1)
+        unit = jnp.where(row == col, 1.0, 0.0).astype(jnp.bfloat16)
+        turned = lax.dot_general(term, unit, (((0,), (0,)), ((), ())), preferred_element_type=jnp.float32)
+        out_ref[:, half:] = turned.astype(jnp.bfloat16)
+
+    return pl.pallas_call(
+        kernel,
+        out_shape=jax.ShapeDtypeStruct((count, half + lanes), jnp.bfloat16),
+        name="prepare",
+    )(tokens, norm_gain[None, :], routes.T, gate_scores.T)
+
+
+def dense(tokens, norm_gain, routes, gate_scores, w_gate, w_up, w_down):
+    width = tokens.shape[1]
+    nexp = lax.axis_size("ep")
+    half = width // 2
+    hidden = w_gate.shape[2]
+    tp = lax.axis_index("tp")
+    first = tp == 0
+    masks = [1 << b for b in reversed(range((nexp - 1).bit_length()))]
+    steps = list(zip(masks, masks[:-2] + masks[-1:] + masks[-2:-1]))
+    lanes = -(-nexp // 128) * 128
+
+    rows = prepare(tokens, norm_gain, routes, gate_scores, lanes)
+
+    def own_first(w, axis):
+        own = lax.dynamic_slice_in_dim(w, tp * half, half, axis)
+        return own, lax.dynamic_slice_in_dim(w, (1 - tp) * half, half, axis)
+
+    gate_own, gate_other = own_first(w_gate[0], 0)
+    up_own, up_other = own_first(w_up[0], 0)
+    in_own = jnp.concatenate([gate_own, up_own], axis=1)
+    in_other = jnp.concatenate([gate_other, up_other], axis=1)
+    down_own, down_other = own_first(w_down[0], 1)
+
+    for mask in steps[:-1]:
+        rows = jnp.concatenate([rows, swap(rows, mask)], axis=0)
+    far = swap(rows, steps[-1])
+    in_own, in_other, down_own, down_other = lax.optimization_barrier(
+        (in_own, in_other, down_own, down_other)
+    )
+    n = rows.shape[0] // 2
+    one, two = rows[n:], far[:n]
+    own = jnp.concatenate(
+        [rows[:n], jnp.where(first, one, two), jnp.where(first, two, one), far[n:]], axis=0
+    )
+    other = swap(own, None)
+    h = jnp.dot(own[:, :half], in_own, preferred_element_type=jnp.float32)
+    h = h + jnp.dot(other[:, :half], in_other, preferred_element_type=jnp.float32)
+    pair = own[:, half:].astype(jnp.float32) + other[:, half:].astype(jnp.float32)
+    mine = (jnp.arange(lanes, dtype=jnp.int32) == lax.axis_index("ep"))[None, :]
+    score = jnp.sum(jnp.where(mine, pair, 0.0), axis=1, keepdims=True)
+    act = clamped_unit(h[:, :hidden], h[:, hidden:]).astype(jnp.bfloat16)
+
+    given = jnp.dot(act, down_other, preferred_element_type=jnp.float32).astype(jnp.bfloat16)
+    taken = swap(given, None)
+    kept = jnp.dot(act, down_own, preferred_element_type=jnp.float32)
+    total = (kept + taken.astype(jnp.float32)) * score
+    one, two = total[n : 2 * n], total[2 * n : 3 * n]
+    near = jnp.concatenate([total[:n], jnp.where(first, one, two)], axis=0)
+    far = jnp.concatenate([jnp.where(first, two, one), total[3 * n :]], axis=0)
+    for mask in reversed(steps):
+        near = near + swap(far.astype(jnp.bfloat16), mask).astype(jnp.float32)
+        n = near.shape[0] // 2
+        if mask is not steps[0]:
+            near, far = near[:n], near[n:]
+    mixed = finish(near)
+    theirs = swap(mixed, None)
+    return jnp.concatenate(
+        [jnp.where(first, mixed, theirs), jnp.where(first, theirs, mixed)], axis=1
+    )
+
+
+def body(tokens, norm_gain, routes, gate_scores, w_gate, w_up, w_down):
+    args = (tokens, norm_gain, routes, gate_scores, w_gate, w_up, w_down)
+    count = tokens.shape[0]
+    top = routes.shape[1]
+    nexp = lax.axis_size("ep")
+    capacity = max(2, min(count, 2 * count * top // nexp))
+    if capacity == count and nexp >= 4 and nexp & (nexp - 1) == 0 and lax.axis_size("tp") == 2:
+        return dense(*args)
+    return slotted(*args, capacity)
+
+
 def solution(mesh):
     in_specs = (
         P(("grp", "ep"), None),

time: 94.4 us -> 43.6 us (0.46)
  blocking collectives: 27.4 us -> 0 us
  waiting for transfers between devices: 38.3 us -> 22.2 us
  between operations: 13.5 us -> 0.19 us
  starting transfers between devices: 5.81 us -> 13.4 us
  matrix products: 3.4 us -> 1.32 us
  Pallas kernels: 0 us -> 1.73 us
  other arithmetic: 3.26 us -> 2.09 us
    all_to_all x1 -> x0, blocking collectives: 27.4 us -> none  [body(): lax.all_to_all(outgoing, 'ep', split_axis=0, concat_axis=0, tiled=True)]
    ppermute x0 -> x9, waiting for transfers between devices: none -> 22.2 us  [the longest x6 18.1 us: swap(): return lax.ppermute(x, ('ep', 'tp'), pairs)]
    all_to_all x1 -> x0, waiting for transfers between devices: 20.2 us -> none  [body(): lax.all_to_all(outputs.reshape(sources, places, outputs.shape[1]), 'ep',...]
    psum x1 -> x0, waiting for transfers between devices: 18.2 us -> none  [expert_rows(): total = lax.psum(part.astype(jnp.bfloat16), 'tp')]
    ppermute x0 -> x9, starting transfers between devices: none -> 13.4 us  [the longest x6 13 us: swap(): return lax.ppermute(x, ('ep', 'tp'), pairs)]
    all_to_all x1 -> x0, starting transfers between devices: 5.81 us -> none  [body(): lax.all_to_all(outputs.reshape(sources, places, outputs.shape[1]), 'ep',...]
    dot_general x3 -> x4, matrix products: 3.4 us -> 1.32 us  [the longest x1 0.39 us: dense(): h = jnp.dot(own[:, :half], in_own, preferred_element_type=jnp.float32)]
    pallas_call x0 -> x1, Pallas kernels: none -> 1.73 us  [prepare(): pl.pallas_call(kernel, out_shape=jax.ShapeDtypeStruct((count, half + lane...]
  transfers between devices with their start and end apart: 2 -> 9, of which waited for: 2 -> 9; matrix products, arithmetic and copies ran while one was open for 0% -> 6% of each run, Pallas kernels for 0% -> 0%
where the time goes in v2:
time: 43.6 us; the launch traced here: 43.3 us
  waiting for transfers between devices  22.2 us (51%)
  starting transfers between devices  13.4 us (31%)
  local copies, waits for them, and re-layouts  2.42 us (6%)
  other arithmetic  2.09 us (5%)
  Pallas kernels  1.73 us (4%)
  matrix products  1.32 us (3%)
    ppermute x6, waiting for transfers between devices, swap(): return lax.ppermute(x, ('ep', 'tp'), pairs)  18.1 us
    ppermute x6, starting transfers between devices, swap(): return lax.ppermute(x, ('ep', 'tp'), pairs)  13 us
    ppermute x3, waiting for transfers between devices, swap(): return lax.ppermute(x, 'tp', [(c, c ^ 1) for c in range(cores)])  4.13 us
    pallas_call x1, Pallas kernels, prepare(): pl.pallas_call(kernel, out_shape=jax.ShapeDtypeStruct((count, half + lane...  1.73 us
    dynamic_slice x2, local copies, waits for them, and re-layouts, own_first(): return (own, lax.dynamic_slice_in_dim(w, (1 - tp) * half, half, axis))  1.5 us
    unnamed x8, local copies, waits for them, and re-layouts  0.88 us
  transfers between devices with their start and end apart: 9, of which 9 were waited for; matrix products, arithmetic and copies ran while one was open for 6% of the time, Pallas kernels for 0%

profile of v2, /device:TPU:0, one launch (start us, length us, event | category | flops | bytes accessed | tf_op | source)
XLA Modules:
  0.0 43.3 jit_solution(9587960274680844413)
XLA Ops:
  0.0 1.7 %prepare.1 = bf16[24,1152]{1,0:T(8,128)(2,1)} custom-call(bf16[24,2048]{1,0:T(8,128)(2,1)} %x_ref.1, f32[1,2048]{1,0:T(1,128)} %bitcast.21, s32[4,24]{1,0:T(4,128)} %bitcast.22, f32[4,24]{1,0:T(4,128)} %bitcast.23), custom_call_target="tpu_custom_call" | custom-call | tf_op jit(solution)/shard_map/prepare/pallas_call | solution.py:114
  1.7 4.1 %collective-permute-start = (bf16[24,1152]{1,0:T(8,128)(2,1)}, bf16[24,1152]{1,0:T(8,128)(2,1)S(1)}, u32[]{:S(2)}, u32[]{:S(2)}) collective-permute-start(bf16[24,1152]{1,0:T(8,128)(2,1)} %prepare.1), channel_id=1, source_target_pairs={{0,8},{1,9},{2,10},{3,11},{4,12},{5,13},{6,14},{7,15},{8,0},{9,1},... | collective-permute-start | bytes 165896 | tf_op jit(solution)/shard_map/ppermute | solution.py:87
  5.8 0.9 %constant_dynamic-update-slice_fusion.1 = bf16[192,1152]{1,0:T(8,128)(2,1)S(1)} fusion(bf16[24,1152]{1,0:T(8,128)(2,1)} %prepare.1), kind=kLoop, calls=%fused_computation.40 | loop fusion | bytes 110592
  6.7 2.1 %collective-permute-done = bf16[24,1152]{1,0:T(8,128)(2,1)S(1)} collective-permute-done((bf16[24,1152]{1,0:T(8,128)(2,1)}, bf16[24,1152]{1,0:T(8,128)(2,1)S(1)}, u32[]{:S(2)}, u32[]{:S(2)}) %collective-permute-start) | collective-permute-done | bytes 55328 | tf_op jit(solution)/shard_map/ppermute | solution.py:87
  8.7 0.8 %pad_maximum_fusion.4 = bf16[48,1152]{1,0:T(8,128)(2,1)S(1)} fusion(bf16[24,1152]{1,0:T(8,128)(2,1)S(1)} %collective-permute-done, bf16[24,1152]{1,0:T(8,128)(2,1)} %prepare.1), kind=kLoop, calls=%fused_computation.29 | loop fusion | flops 221184 | bytes 221184 | tf_op jit(solution)/shard_map/concatenate | solution.py:145
  9.6 0.0 copy-start.2
  9.6 1.4 %collective-permute-start.1 = (bf16[48,1152]{1,0:T(8,128)(2,1)S(1)}, bf16[48,1152]{1,0:T(8,128)(2,1)S(1)}, u32[]{:S(2)}, u32[]{:S(2)}) collective-permute-start(bf16[48,1152]{1,0:T(8,128)(2,1)S(1)} %pad_maximum_fusion.4), channel_id=1, source_target_pairs={{0,4},{1,3},{2,6},{3,1},{4,0},{5,7},{6,2},{7,5},{8,12},{9,11},{10,... | collective-permute-start | bytes 331784 | tf_op jit(solution)/shard_map/ppermute | solution.py:87
  11.0 0.0 copy-start.1
  11.0 1.4 %dynamic-slice_bitcast_fusion = (bf16[256,1024]{1,0:T(8,128)(2,1)S(1)}, bf16[256,1024]{1,0:T(8,128)(2,1)S(1)}) fusion(bf16[1,256,2048]{2,1,0:T(8,128)(2,1)} %param.13, s32[]{:T(128)S(6)} %select_n.55, s32[]{:T(128)S(6)} %select_n.54), kind=kLoop, calls=%fused_computation.5 | loop fusion | bytes 2097160 | tf_op jit(solution)/shard_map/dynamic_slice | solution.py:136
  12.3 0.0 copy-start
  12.3 2.1 %collective-permute-done.1 = bf16[48,1152]{1,0:T(8,128)(2,1)S(1)} collective-permute-done((bf16[48,1152]{1,0:T(8,128)(2,1)S(1)}, bf16[48,1152]{1,0:T(8,128)(2,1)S(1)}, u32[]{:S(2)}, u32[]{:S(2)}) %collective-permute-start.1) | collective-permute-done | bytes 110624 | tf_op jit(solution)/shard_map/ppermute | solution.py:87
  14.5 0.0 copy-done.2
  14.5 2.0 %collective-permute-start.2 = (bf16[96,1152]{1,0:T(8,128)(2,1)S(1)}, bf16[96,1152]{1,0:T(8,128)(2,1)S(1)}, u32[]{:S(2)}, u32[]{:S(2)}) collective-permute-start(bf16[96,1152]{1,0:T(8,128)(2,1)S(1)} %pad_maximum_fusion.2), channel_id=1, source_target_pairs={{0,2},{1,5},{2,0},{3,7},{4,6},{5,1},{6,4},{7,3},{8,10},{9,13},{10,... | collective-permute-start | bytes 663560 | tf_op jit(solution)/shard_map/ppermute | solution.py:87
  16.5 4.0 %collective-permute-done.2 = bf16[96,1152]{1,0:T(8,128)(2,1)S(1)} collective-permute-done((bf16[96,1152]{1,0:T(8,128)(2,1)S(1)}, bf16[96,1152]{1,0:T(8,128)(2,1)S(1)}, u32[]{:S(2)}, u32[]{:S(2)}) %collective-permute-start.2) | collective-permute-done | bytes 221216 | tf_op jit(solution)/shard_map/ppermute | solution.py:87
  20.6 0.1 collective-permute-start.3
  20.7 0.0 copy-done.1
  20.7 0.0 copy-done
  20.7 0.1 dynamic-slice_bitcast_fusion.2
  20.8 0.1 pad_maximum_fusion
  20.9 0.1 pad_maximum_fusion.1
  21.0 1.4 %collective-permute-done.3 = bf16[192,1152]{1,0:T(8,128)(2,1)S(1)} collective-permute-done((bf16[192,1152]{1,0:T(8,128)(2,1)S(1)}, bf16[192,1152]{1,0:T(8,128)(2,1)S(1)}, u32[]{:S(2)}, u32[]{:S(2)}) %collective-permute-start.3) | collective-permute-done | bytes 442400 | tf_op jit(solution)/shard_map/ppermute | solution.py:85
  22.5 0.4 fusion
  22.8 0.4 convolution_add_fusion
  23.2 0.1 fusion.6
  23.3 0.3 convolution_convert_fusion
  23.6 0.2 collective-permute-start.4
  23.8 0.1 select_reduce_fusion
  23.9 1.5 %collective-permute-done.4 = bf16[192,1024]{1,0:T(8,128)(2,1)S(1)} collective-permute-done((bf16[192,1024]{1,0:T(8,128)(2,1)S(1)}, bf16[192,1024]{1,0:T(8,128)(2,1)S(1)}, u32[]{:S(2)}, u32[]{:S(2)}) %collective-permute-start.4) | collective-permute-done | bytes 393248 | tf_op jit(solution)/shard_map/ppermute | solution.py:85
  25.4 0.3 add_multiply_fusion
  25.7 1.9 %collective-permute-start.5 = (bf16[96,1024]{1,0:T(8,128)(2,1)S(1)}, bf16[96,1024]{1,0:T(8,128)(2,1)S(1)}, u32[]{:S(2)}, u32[]{:S(2)}) collective-permute-start(bf16[96,1024]{1,0:T(8,128)(2,1)S(1)} %pad_maximum_fusion.3), channel_id=1, source_target_pairs={{0,2},{1,5},{2,0},{3,7},{4,6},{5,1},{6,4},{7,3},{8,10},{9,13},{10,... | collective-permute-start | bytes 589832 | tf_op jit(solution)/shard_map/ppermute | solution.py:87
  27.7 3.8 %collective-permute-done.5 = bf16[96,1024]{1,0:T(8,128)(2,1)S(1)} collective-permute-done((bf16[96,1024]{1,0:T(8,128)(2,1)S(1)}, bf16[96,1024]{1,0:T(8,128)(2,1)S(1)}, u32[]{:S(2)}, u32[]{:S(2)}) %collective-permute-start.5) | collective-permute-done | bytes 196640 | tf_op jit(solution)/shard_map/ppermute | solution.py:87
  31.5 1.3 %collective-permute-start.6 = (bf16[48,1024]{1,0:T(8,128)(2,1)S(1)}, bf16[48,1024]{1,0:T(8,128)(2,1)S(1)}, u32[]{:S(2)}, u32[]{:S(2)}) collective-permute-start(bf16[48,1024]{1,0:T(8,128)(2,1)S(1)} %slice.115), channel_id=1, source_target_pairs={{0,4},{1,3},{2,6},{3,1},{4,0},{5,7},{6,2},{7,5},{8,12},{9,11},{10,... | collective-permute-start | bytes 294920 | tf_op jit(solution)/shard_map/ppermute | solution.py:87
  32.8 3.4 %collective-permute-done.6 = bf16[48,1024]{1,0:T(8,128)(2,1)S(1)} collective-permute-done((bf16[48,1024]{1,0:T(8,128)(2,1)S(1)}, bf16[48,1024]{1,0:T(8,128)(2,1)S(1)}, u32[]{:S(2)}, u32[]{:S(2)}) %collective-permute-start.6) | collective-permute-done | bytes 98336 | tf_op jit(solution)/shard_map/ppermute | solution.py:87
  36.3 2.4 %collective-permute-start.7 = (bf16[24,1024]{1,0:T(8,128)(2,1)S(1)}, bf16[24,1024]{1,0:T(8,128)(2,1)S(1)}, u32[]{:S(2)}, u32[]{:S(2)}) collective-permute-start(bf16[24,1024]{1,0:T(8,128)(2,1)S(1)} %slice.117), channel_id=1, source_target_pairs={{0,8},{1,9},{2,10},{3,11},{4,12},{5,13},{6,14},{7,15},{8,0},{9,1},... | collective-permute-start | bytes 147464 | tf_op jit(solution)/shard_map/ppermute | solution.py:87
  38.7 2.6 %collective-permute-done.7 = bf16[24,1024]{1,0:T(8,128)(2,1)S(1)} collective-permute-done((bf16[24,1024]{1,0:T(8,128)(2,1)S(1)}, bf16[24,1024]{1,0:T(8,128)(2,1)S(1)}, u32[]{:S(2)}, u32[]{:S(2)}) %collective-permute-start.7) | collective-permute-done | bytes 49184 | tf_op jit(solution)/shard_map/ppermute | solution.py:87
  41.3 0.1 collective-permute-start.8
  41.4 1.2 %collective-permute-done.8 = bf16[24,1024]{1,0:T(8,128)(2,1)S(1)} collective-permute-done((bf16[24,1024]{1,0:T(8,128)(2,1)S(1)}, bf16[24,1024]{1,0:T(8,128)(2,1)S(1)}, u32[]{:S(2)}, u32[]{:S(2)}) %collective-permute-start.8) | collective-permute-done | bytes 49184 | tf_op jit(solution)/shard_map/ppermute | solution.py:85
  42.6 0.6 %pad_maximum_fusion.5 = bf16[24,2048]{1,0:T(8,128)(2,1)} fusion(bf16[24,1024]{1,0:T(8,128)(2,1)S(1)} %get-tuple-element.24, bf16[24,1024]{1,0:T(8,128)(2,1)S(1)} %get-tuple-element.23), kind=kLoop, calls=%fused_computation.35 | loop fusion | flops 196608 | bytes 196608 | tf_op jit(solution)/shard_map/concatenate | solution.py:177
  (15 shorter events, 0.3 us)
Async XLA Ops:
  1.7 7.0 %collective-permute-start = (bf16[24,1152]{1,0:T(8,128)(2,1)}, bf16[24,1152]{1,0:T(8,128)(2,1)S(1)}, u32[]{:S(2)}, u32[]{:S(2)}) collective-permute-start(bf16[24,1152]{1,0:T(8,128)(2,1)} %prepare.1), channel_id=1, source_target_pairs={{0,8},{1,9},{2,10},{3,11},{4,12},{5,13},{6,14},{7,15},{8,0},{9,1},... | collective-permute-start | bytes 165896 | tf_op jit(solution)/shard_map/ppermute | solution.py:87
  9.6 4.9 %copy-start.2 = (bf16[24,1152]{1,0:T(8,128)(2,1)S(1)}, bf16[24,1152]{1,0:T(8,128)(2,1)}, u32[]{:S(2)}) copy-start(bf16[24,1152]{1,0:T(8,128)(2,1)} %prepare.1) | copy-start | bytes 165892
  9.6 4.9 %collective-permute-start.1 = (bf16[48,1152]{1,0:T(8,128)(2,1)S(1)}, bf16[48,1152]{1,0:T(8,128)(2,1)S(1)}, u32[]{:S(2)}, u32[]{:S(2)}) collective-permute-start(bf16[48,1152]{1,0:T(8,128)(2,1)S(1)} %pad_maximum_fusion.4), channel_id=1, source_target_pairs={{0,4},{1,3},{2,6},{3,1},{4,0},{5,7},{6,2},{7,5},{8,12},{9,11},{10,... | collective-permute-start | bytes 331784 | tf_op jit(solution)/shard_map/ppermute | solution.py:87
  11.0 9.7 %copy-start.1 = (bf16[1,2048,256]{2,1,0:T(8,128)(2,1)S(1)}, bf16[1,2048,256]{2,1,0:T(8,128)(2,1)}, u32[]{:S(2)}) copy-start(bf16[1,2048,256]{2,1,0:T(8,128)(2,1)} %param.11) | copy-start | bytes 3145732
  12.3 8.4 %copy-start = (bf16[1,2048,256]{2,1,0:T(8,128)(2,1)S(1)}, bf16[1,2048,256]{2,1,0:T(8,128)(2,1)}, u32[]{:S(2)}) copy-start(bf16[1,2048,256]{2,1,0:T(8,128)(2,1)} %param.12) | copy-start | bytes 3145732
  14.5 6.0 %collective-permute-start.2 = (bf16[96,1152]{1,0:T(8,128)(2,1)S(1)}, bf16[96,1152]{1,0:T(8,128)(2,1)S(1)}, u32[]{:S(2)}, u32[]{:S(2)}) collective-permute-start(bf16[96,1152]{1,0:T(8,128)(2,1)S(1)} %pad_maximum_fusion.2), channel_id=1, source_target_pairs={{0,2},{1,5},{2,0},{3,7},{4,6},{5,1},{6,4},{7,3},{8,10},{9,13},{10,... | collective-permute-start | bytes 663560 | tf_op jit(solution)/shard_map/ppermute | solution.py:87
  20.6 1.9 %collective-permute-start.3 = (bf16[192,1152]{1,0:T(8,128)(2,1)S(1)}, bf16[192,1152]{1,0:T(8,128)(2,1)S(1)}, u32[]{:S(2)}, u32[]{:S(2)}) collective-permute-start(bf16[192,1152]{1,0:T(8,128)(2,1)S(1)} %slice_dynamic-update-slice_fusion), channel_id=1, source_target_pairs={{0,1},{1,0},{2,3},{3,2},{4,5},{5,4},{6,7},{7,6},{8,9},{9,8},{10,11... | collective-permute-start | bytes 1327112 | tf_op jit(solution)/shard_map/ppermute | solution.py:85
  23.6 1.8 %collective-permute-start.4 = (bf16[192,1024]{1,0:T(8,128)(2,1)S(1)}, bf16[192,1024]{1,0:T(8,128)(2,1)S(1)}, u32[]{:S(2)}, u32[]{:S(2)}) collective-permute-start(bf16[192,1024]{1,0:T(8,128)(2,1)S(1)} %convolution_convert_fusion), channel_id=1, source_target_pairs={{0,1},{1,0},{2,3},{3,2},{4,5},{5,4},{6,7},{7,6},{8,9},{9,8},{10,11... | collective-permute-start | bytes 1179656 | tf_op jit(solution)/shard_map/ppermute | solution.py:85
  25.7 5.7 %collective-permute-start.5 = (bf16[96,1024]{1,0:T(8,128)(2,1)S(1)}, bf16[96,1024]{1,0:T(8,128)(2,1)S(1)}, u32[]{:S(2)}, u32[]{:S(2)}) collective-permute-start(bf16[96,1024]{1,0:T(8,128)(2,1)S(1)} %pad_maximum_fusion.3), channel_id=1, source_target_pairs={{0,2},{1,5},{2,0},{3,7},{4,6},{5,1},{6,4},{7,3},{8,10},{9,13},{10,... | collective-permute-start | bytes 589832 | tf_op jit(solution)/shard_map/ppermute | solution.py:87
  31.5 4.7 %collective-permute-start.6 = (bf16[48,1024]{1,0:T(8,128)(2,1)S(1)}, bf16[48,1024]{1,0:T(8,128)(2,1)S(1)}, u32[]{:S(2)}, u32[]{:S(2)}) collective-permute-start(bf16[48,1024]{1,0:T(8,128)(2,1)S(1)} %slice.115), channel_id=1, source_target_pairs={{0,4},{1,3},{2,6},{3,1},{4,0},{5,7},{6,2},{7,5},{8,12},{9,11},{10,... | collective-permute-start | bytes 294920 | tf_op jit(solution)/shard_map/ppermute | solution.py:87
  36.3 5.1 %collective-permute-start.7 = (bf16[24,1024]{1,0:T(8,128)(2,1)S(1)}, bf16[24,1024]{1,0:T(8,128)(2,1)S(1)}, u32[]{:S(2)}, u32[]{:S(2)}) collective-permute-start(bf16[24,1024]{1,0:T(8,128)(2,1)S(1)} %slice.117), channel_id=1, source_target_pairs={{0,8},{1,9},{2,10},{3,11},{4,12},{5,13},{6,14},{7,15},{8,0},{9,1},... | collective-permute-start | bytes 147464 | tf_op jit(solution)/shard_map/ppermute | solution.py:87
  41.3 1.3 %collective-permute-start.8 = (bf16[24,1024]{1,0:T(8,128)(2,1)S(1)}, bf16[24,1024]{1,0:T(8,128)(2,1)S(1)}, u32[]{:S(2)}, u32[]{:S(2)}) collective-permute-start(bf16[24,1024]{1,0:T(8,128)(2,1)S(1)} %fusion.7), channel_id=1, source_target_pairs={{0,1},{1,0},{2,3},{3,2},{4,5},{5,4},{6,7},{7,6},{8,9},{9,8},{10,11... | collective-permute-start | bytes 147464 | tf_op jit(solution)/shard_map/ppermute | solution.py:85

commit v3 on v2

--- a/solution.py
+++ b/solution.py
@@ -2,6 +2,7 @@
 import jax.numpy as jnp
 from jax import lax
 from jax.experimental import pallas as pl
+from jax.experimental.pallas import tpu as pltpu
 from jax.sharding import PartitionSpec as P
 
 
@@ -113,7 +114,8 @@
 
     return pl.pallas_call(
         kernel,
-        out_shape=jax.ShapeDtypeStruct((count, half + lanes), jnp.bfloat16),
+        out_shape=pltpu.VMEM((count, half + lanes), jnp.bfloat16),
+        compiler_params=pltpu.CompilerParams(vmem_limit_bytes=4 << 20),
         name="prepare",
     )(tokens, norm_gain[None, :], routes.T, gate_scores.T)
 

time: 43.6 us -> 44 us (level)
  local copies, waits for them, and re-layouts: 2.42 us -> 4.52 us
  Pallas kernels: 1.73 us -> 0.2 us
  other arithmetic: 2.09 us -> 1.27 us
  waiting for transfers between devices: 22.2 us -> 22.8 us
    unnamed x8 -> x14, local copies, waits for them, and re-layouts: 0.88 us -> 2.98 us
    pallas_call x1, Pallas kernels: 1.73 us -> 0.2 us  [prepare(): pl.pallas_call(kernel, out_shape=pltpu.VMEM((count, half + lanes), jnp.bf...]
    concatenate x2, other arithmetic: 0.84 us -> 0.03 us  [dense(): rows = jnp.concatenate([rows, swap(rows, mask)], axis=0)]
    ppermute x6, waiting for transfers between devices: 18.1 us -> 18.7 us  [swap(): return lax.ppermute(x, ('ep', 'tp'), pairs)]
  transfers between devices with their start and end apart: 9 -> 9, of which waited for: 9 -> 9; matrix products, arithmetic and copies ran while one was open for 6% -> 4% of each run, Pallas kernels for 0% -> 0%
where the time goes in v3:
time: 44 us; the launch traced here: 43.7 us
  waiting for transfers between devices  22.8 us (52%)
  starting transfers between devices  13.4 us (30%)
  local copies, waits for them, and re-layouts  4.52 us (10%)
  matrix products  1.29 us (3%)
  other arithmetic  1.27 us (3%)
    ppermute x6, waiting for transfers between devices, swap(): return lax.ppermute(x, ('ep', 'tp'), pairs)  18.7 us
    ppermute x6, starting transfers between devices, swap(): return lax.ppermute(x, ('ep', 'tp'), pairs)  13.1 us
    ppermute x3, waiting for transfers between devices, swap(): return lax.ppermute(x, 'tp', [(c, c ^ 1) for c in range(cores)])  4.12 us
    unnamed x14, local copies, waits for them, and re-layouts  2.98 us
    dynamic_slice x2, local copies, waits for them, and re-layouts, own_first(): return (own, lax.dynamic_slice_in_dim(w, (1 - tp) * half, half, axis))  1.5 us
  transfers between devices with their start and end apart: 9, of which 9 were waited for; matrix products, arithmetic and copies ran while one was open for 4% of the time, Pallas kernels for 0%

profile of v3, /device:TPU:0, one launch (start us, length us, event | category | flops | bytes accessed | tf_op | source)
XLA Modules:
  0.0 43.7 jit_solution(6686418533183174038)
XLA Ops:
  0.0 0.0 copy-start
  0.0 0.9 %copy-done = bf16[24,2048]{1,0:T(8,128)(2,1)S(1)} copy-done((bf16[24,2048]{1,0:T(8,128)(2,1)S(1)}, bf16[24,2048]{1,0:T(8,128)(2,1)}, u32[]{:S(2)}) %copy-start) | copy-done | bytes 98328
  0.9 0.0 copy-start.1
  0.9 0.7 %copy-done.1 = f32[2048]{0:T(1024)S(1)} copy-done((f32[2048]{0:T(1024)S(1)}, f32[2048]{0:T(1024)}, u32[]{:S(2)}) %copy-start.1) | copy-done | bytes 8216
  1.6 0.0 copy-start.2
  1.6 0.7 %copy-done.2 = s32[24,4]{0,1:T(4,128)S(1)} copy-done((s32[24,4]{0,1:T(4,128)S(1)}, s32[24,4]{0,1:T(4,128)}, u32[]{:S(2)}) %copy-start.2) | copy-done | bytes 408
  2.3 0.0 copy-start.3
  2.3 0.7 %copy-done.3 = f32[24,4]{0,1:T(4,128)S(1)} copy-done((f32[24,4]{0,1:T(4,128)S(1)}, f32[24,4]{0,1:T(4,128)}, u32[]{:S(2)}) %copy-start.3) | copy-done | bytes 408
  3.0 0.2 prepare.1
  3.2 4.1 %collective-permute-start = (bf16[24,1152]{1,0:T(8,128)(2,1)S(1)}, bf16[24,1152]{1,0:T(8,128)(2,1)S(1)}, u32[]{:S(2)}, u32[]{:S(2)}) collective-permute-start(bf16[24,1152]{1,0:T(8,128)(2,1)S(1)} %prepare.1), channel_id=1, source_target_pairs={{0,8},{1,9},{2,10},{3,11},{4,12},{5,13},{6,14},{7,15},{8,0},{9,1},... | collective-permute-start | bytes 165896 | tf_op jit(solution)/shard_map/ppermute | solution.py:88
  7.3 2.7 %collective-permute-done = bf16[24,1152]{1,0:T(8,128)(2,1)S(1)} collective-permute-done((bf16[24,1152]{1,0:T(8,128)(2,1)S(1)}, bf16[24,1152]{1,0:T(8,128)(2,1)S(1)}, u32[]{:S(2)}, u32[]{:S(2)}) %collective-permute-start) | collective-permute-done | bytes 55328 | tf_op jit(solution)/shard_map/ppermute | solution.py:88
  10.0 1.4 %collective-permute-start.1 = (bf16[48,1152]{1,0:T(8,128)(2,1)S(1)}, bf16[48,1152]{1,0:T(8,128)(2,1)S(1)}, u32[]{:S(2)}, u32[]{:S(2)}) collective-permute-start(bf16[48,1152]{1,0:T(8,128)(2,1)S(1)} %pad_maximum_fusion.4), channel_id=1, source_target_pairs={{0,4},{1,3},{2,6},{3,1},{4,0},{5,7},{6,2},{7,5},{8,12},{9,11},{10,... | collective-permute-start | bytes 331784 | tf_op jit(solution)/shard_map/ppermute | solution.py:88
  11.4 0.0 copy-start.5
  11.4 1.4 %dynamic-slice_bitcast_fusion = (bf16[256,1024]{1,0:T(8,128)(2,1)S(1)}, bf16[256,1024]{1,0:T(8,128)(2,1)S(1)}) fusion(bf16[1,256,2048]{2,1,0:T(8,128)(2,1)} %param.13, s32[]{:T(128)S(6)} %select_n.55, s32[]{:T(128)S(6)} %select_n.54), kind=kLoop, calls=%fused_computation.5 | loop fusion | bytes 2097160 | tf_op jit(solution)/shard_map/dynamic_slice | solution.py:138
  12.7 0.0 copy-start.4
  12.7 2.2 %collective-permute-done.1 = bf16[48,1152]{1,0:T(8,128)(2,1)S(1)} collective-permute-done((bf16[48,1152]{1,0:T(8,128)(2,1)S(1)}, bf16[48,1152]{1,0:T(8,128)(2,1)S(1)}, u32[]{:S(2)}, u32[]{:S(2)}) %collective-permute-start.1) | collective-permute-done | bytes 110624 | tf_op jit(solution)/shard_map/ppermute | solution.py:88
  14.9 1.9 %collective-permute-start.2 = (bf16[96,1152]{1,0:T(8,128)(2,1)S(1)}, bf16[96,1152]{1,0:T(8,128)(2,1)S(1)}, u32[]{:S(2)}, u32[]{:S(2)}) collective-permute-start(bf16[96,1152]{1,0:T(8,128)(2,1)S(1)} %pad_maximum_fusion.2), channel_id=1, source_target_pairs={{0,2},{1,5},{2,0},{3,7},{4,6},{5,1},{6,4},{7,3},{8,10},{9,13},{10,... | collective-permute-start | bytes 663560 | tf_op jit(solution)/shard_map/ppermute | solution.py:88
  16.9 4.0 %collective-permute-done.2 = bf16[96,1152]{1,0:T(8,128)(2,1)S(1)} collective-permute-done((bf16[96,1152]{1,0:T(8,128)(2,1)S(1)}, bf16[96,1152]{1,0:T(8,128)(2,1)S(1)}, u32[]{:S(2)}, u32[]{:S(2)}) %collective-permute-start.2) | collective-permute-done | bytes 221216 | tf_op jit(solution)/shard_map/ppermute | solution.py:88
  21.0 0.1 collective-permute-start.3
  21.1 0.0 copy-done.5
  21.1 0.0 copy-done.4
  21.1 0.1 dynamic-slice_bitcast_fusion.2
  21.3 0.1 pad_maximum_fusion
  21.4 0.1 pad_maximum_fusion.1
  21.4 1.4 %collective-permute-done.3 = bf16[192,1152]{1,0:T(8,128)(2,1)S(1)} collective-permute-done((bf16[192,1152]{1,0:T(8,128)(2,1)S(1)}, bf16[192,1152]{1,0:T(8,128)(2,1)S(1)}, u32[]{:S(2)}, u32[]{:S(2)}) %collective-permute-start.3) | collective-permute-done | bytes 442400 | tf_op jit(solution)/shard_map/ppermute | solution.py:86
  22.9 0.4 fusion
  23.3 0.4 convolution_add_fusion
  23.6 0.1 fusion.6
  23.7 0.3 convolution_convert_fusion
  24.0 0.2 collective-permute-start.4
  24.2 0.1 select_reduce_fusion
  24.3 1.5 %collective-permute-done.4 = bf16[192,1024]{1,0:T(8,128)(2,1)S(1)} collective-permute-done((bf16[192,1024]{1,0:T(8,128)(2,1)S(1)}, bf16[192,1024]{1,0:T(8,128)(2,1)S(1)}, u32[]{:S(2)}, u32[]{:S(2)}) %collective-permute-start.4) | collective-permute-done | bytes 393248 | tf_op jit(solution)/shard_map/ppermute | solution.py:86
  25.8 0.3 add_multiply_fusion
  26.1 2.0 %collective-permute-start.5 = (bf16[96,1024]{1,0:T(8,128)(2,1)S(1)}, bf16[96,1024]{1,0:T(8,128)(2,1)S(1)}, u32[]{:S(2)}, u32[]{:S(2)}) collective-permute-start(bf16[96,1024]{1,0:T(8,128)(2,1)S(1)} %pad_maximum_fusion.3), channel_id=1, source_target_pairs={{0,2},{1,5},{2,0},{3,7},{4,6},{5,1},{6,4},{7,3},{8,10},{9,13},{10,... | collective-permute-start | bytes 589832 | tf_op jit(solution)/shard_map/ppermute | solution.py:88
  28.1 3.7 %collective-permute-done.5 = bf16[96,1024]{1,0:T(8,128)(2,1)S(1)} collective-permute-done((bf16[96,1024]{1,0:T(8,128)(2,1)S(1)}, bf16[96,1024]{1,0:T(8,128)(2,1)S(1)}, u32[]{:S(2)}, u32[]{:S(2)}) %collective-permute-start.5) | collective-permute-done | bytes 196640 | tf_op jit(solution)/shard_map/ppermute | solution.py:88
  31.9 1.3 %collective-permute-start.6 = (bf16[48,1024]{1,0:T(8,128)(2,1)S(1)}, bf16[48,1024]{1,0:T(8,128)(2,1)S(1)}, u32[]{:S(2)}, u32[]{:S(2)}) collective-permute-start(bf16[48,1024]{1,0:T(8,128)(2,1)S(1)} %slice.115), channel_id=1, source_target_pairs={{0,4},{1,3},{2,6},{3,1},{4,0},{5,7},{6,2},{7,5},{8,12},{9,11},{10,... | collective-permute-start | bytes 294920 | tf_op jit(solution)/shard_map/ppermute | solution.py:88
  33.2 3.4 %collective-permute-done.6 = bf16[48,1024]{1,0:T(8,128)(2,1)S(1)} collective-permute-done((bf16[48,1024]{1,0:T(8,128)(2,1)S(1)}, bf16[48,1024]{1,0:T(8,128)(2,1)S(1)}, u32[]{:S(2)}, u32[]{:S(2)}) %collective-permute-start.6) | collective-permute-done | bytes 98336 | tf_op jit(solution)/shard_map/ppermute | solution.py:88
  36.7 2.4 %collective-permute-start.7 = (bf16[24,1024]{1,0:T(8,128)(2,1)S(1)}, bf16[24,1024]{1,0:T(8,128)(2,1)S(1)}, u32[]{:S(2)}, u32[]{:S(2)}) collective-permute-start(bf16[24,1024]{1,0:T(8,128)(2,1)S(1)} %slice.117), channel_id=1, source_target_pairs={{0,8},{1,9},{2,10},{3,11},{4,12},{5,13},{6,14},{7,15},{8,0},{9,1},... | collective-permute-start | bytes 147464 | tf_op jit(solution)/shard_map/ppermute | solution.py:88
  39.1 2.6 %collective-permute-done.7 = bf16[24,1024]{1,0:T(8,128)(2,1)S(1)} collective-permute-done((bf16[24,1024]{1,0:T(8,128)(2,1)S(1)}, bf16[24,1024]{1,0:T(8,128)(2,1)S(1)}, u32[]{:S(2)}, u32[]{:S(2)}) %collective-permute-start.7) | collective-permute-done | bytes 49184 | tf_op jit(solution)/shard_map/ppermute | solution.py:88
  41.7 0.1 collective-permute-start.8
  41.8 1.2 %collective-permute-done.8 = bf16[24,1024]{1,0:T(8,128)(2,1)S(1)} collective-permute-done((bf16[24,1024]{1,0:T(8,128)(2,1)S(1)}, bf16[24,1024]{1,0:T(8,128)(2,1)S(1)}, u32[]{:S(2)}, u32[]{:S(2)}) %collective-permute-start.8) | collective-permute-done | bytes 49184 | tf_op jit(solution)/shard_map/ppermute | solution.py:86
  43.0 0.6 %pad_maximum_fusion.5 = bf16[24,2048]{1,0:T(8,128)(2,1)} fusion(bf16[24,1024]{1,0:T(8,128)(2,1)S(1)} %get-tuple-element.24, bf16[24,1024]{1,0:T(8,128)(2,1)S(1)} %get-tuple-element.23), kind=kLoop, calls=%fused_computation.35 | loop fusion | flops 196608 | bytes 196608 | tf_op jit(solution)/shard_map/concatenate | solution.py:179
  (17 shorter events, 0.3 us)
Async XLA Ops:
  0.0 0.9 %copy-start = (bf16[24,2048]{1,0:T(8,128)(2,1)S(1)}, bf16[24,2048]{1,0:T(8,128)(2,1)}, u32[]{:S(2)}) copy-start(bf16[24,2048]{1,0:T(8,128)(2,1)} %x_ref.1) | copy-start | bytes 294916
  0.9 0.7 %copy-start.1 = (f32[2048]{0:T(1024)S(1)}, f32[2048]{0:T(1024)}, u32[]{:S(2)}) copy-start(f32[2048]{0:T(1024)} %param.8) | copy-start | bytes 24580
  1.6 0.7 %copy-start.2 = (s32[24,4]{0,1:T(4,128)S(1)}, s32[24,4]{0,1:T(4,128)}, u32[]{:S(2)}) copy-start(s32[24,4]{0,1:T(4,128)} %param.9) | copy-start | bytes 1156
  2.3 0.7 %copy-start.3 = (f32[24,4]{0,1:T(4,128)S(1)}, f32[24,4]{0,1:T(4,128)}, u32[]{:S(2)}) copy-start(f32[24,4]{0,1:T(4,128)} %param.10) | copy-start | bytes 1156
  3.2 6.8 %collective-permute-start = (bf16[24,1152]{1,0:T(8,128)(2,1)S(1)}, bf16[24,1152]{1,0:T(8,128)(2,1)S(1)}, u32[]{:S(2)}, u32[]{:S(2)}) collective-permute-start(bf16[24,1152]{1,0:T(8,128)(2,1)S(1)} %prepare.1), channel_id=1, source_target_pairs={{0,8},{1,9},{2,10},{3,11},{4,12},{5,13},{6,14},{7,15},{8,0},{9,1},... | collective-permute-start | bytes 165896 | tf_op jit(solution)/shard_map/ppermute | solution.py:88
  10.0 4.9 %collective-permute-start.1 = (bf16[48,1152]{1,0:T(8,128)(2,1)S(1)}, bf16[48,1152]{1,0:T(8,128)(2,1)S(1)}, u32[]{:S(2)}, u32[]{:S(2)}) collective-permute-start(bf16[48,1152]{1,0:T(8,128)(2,1)S(1)} %pad_maximum_fusion.4), channel_id=1, source_target_pairs={{0,4},{1,3},{2,6},{3,1},{4,0},{5,7},{6,2},{7,5},{8,12},{9,11},{10,... | collective-permute-start | bytes 331784 | tf_op jit(solution)/shard_map/ppermute | solution.py:88
  11.4 9.7 %copy-start.5 = (bf16[1,2048,256]{2,1,0:T(8,128)(2,1)S(1)}, bf16[1,2048,256]{2,1,0:T(8,128)(2,1)}, u32[]{:S(2)}) copy-start(bf16[1,2048,256]{2,1,0:T(8,128)(2,1)} %param.11) | copy-start | bytes 3145732
  12.7 8.4 %copy-start.4 = (bf16[1,2048,256]{2,1,0:T(8,128)(2,1)S(1)}, bf16[1,2048,256]{2,1,0:T(8,128)(2,1)}, u32[]{:S(2)}) copy-start(bf16[1,2048,256]{2,1,0:T(8,128)(2,1)} %param.12) | copy-start | bytes 3145732
  14.9 6.0 %collective-permute-start.2 = (bf16[96,1152]{1,0:T(8,128)(2,1)S(1)}, bf16[96,1152]{1,0:T(8,128)(2,1)S(1)}, u32[]{:S(2)}, u32[]{:S(2)}) collective-permute-start(bf16[96,1152]{1,0:T(8,128)(2,1)S(1)} %pad_maximum_fusion.2), channel_id=1, source_target_pairs={{0,2},{1,5},{2,0},{3,7},{4,6},{5,1},{6,4},{7,3},{8,10},{9,13},{10,... | collective-permute-start | bytes 663560 | tf_op jit(solution)/shard_map/ppermute | solution.py:88
  21.0 1.9 %collective-permute-start.3 = (bf16[192,1152]{1,0:T(8,128)(2,1)S(1)}, bf16[192,1152]{1,0:T(8,128)(2,1)S(1)}, u32[]{:S(2)}, u32[]{:S(2)}) collective-permute-start(bf16[192,1152]{1,0:T(8,128)(2,1)S(1)} %slice_dynamic-update-slice_fusion), channel_id=1, source_target_pairs={{0,1},{1,0},{2,3},{3,2},{4,5},{5,4},{6,7},{7,6},{8,9},{9,8},{10,11... | collective-permute-start | bytes 1327112 | tf_op jit(solution)/shard_map/ppermute | solution.py:86
  24.0 1.8 %collective-permute-start.4 = (bf16[192,1024]{1,0:T(8,128)(2,1)S(1)}, bf16[192,1024]{1,0:T(8,128)(2,1)S(1)}, u32[]{:S(2)}, u32[]{:S(2)}) collective-permute-start(bf16[192,1024]{1,0:T(8,128)(2,1)S(1)} %convolution_convert_fusion), channel_id=1, source_target_pairs={{0,1},{1,0},{2,3},{3,2},{4,5},{5,4},{6,7},{7,6},{8,9},{9,8},{10,11... | collective-permute-start | bytes 1179656 | tf_op jit(solution)/shard_map/ppermute | solution.py:86
  26.1 5.7 %collective-permute-start.5 = (bf16[96,1024]{1,0:T(8,128)(2,1)S(1)}, bf16[96,1024]{1,0:T(8,128)(2,1)S(1)}, u32[]{:S(2)}, u32[]{:S(2)}) collective-permute-start(bf16[96,1024]{1,0:T(8,128)(2,1)S(1)} %pad_maximum_fusion.3), channel_id=1, source_target_pairs={{0,2},{1,5},{2,0},{3,7},{4,6},{5,1},{6,4},{7,3},{8,10},{9,13},{10,... | collective-permute-start | bytes 589832 | tf_op jit(solution)/shard_map/ppermute | solution.py:88
  31.9 4.7 %collective-permute-start.6 = (bf16[48,1024]{1,0:T(8,128)(2,1)S(1)}, bf16[48,1024]{1,0:T(8,128)(2,1)S(1)}, u32[]{:S(2)}, u32[]{:S(2)}) collective-permute-start(bf16[48,1024]{1,0:T(8,128)(2,1)S(1)} %slice.115), channel_id=1, source_target_pairs={{0,4},{1,3},{2,6},{3,1},{4,0},{5,7},{6,2},{7,5},{8,12},{9,11},{10,... | collective-permute-start | bytes 294920 | tf_op jit(solution)/shard_map/ppermute | solution.py:88
  36.7 5.1 %collective-permute-start.7 = (bf16[24,1024]{1,0:T(8,128)(2,1)S(1)}, bf16[24,1024]{1,0:T(8,128)(2,1)S(1)}, u32[]{:S(2)}, u32[]{:S(2)}) collective-permute-start(bf16[24,1024]{1,0:T(8,128)(2,1)S(1)} %slice.117), channel_id=1, source_target_pairs={{0,8},{1,9},{2,10},{3,11},{4,12},{5,13},{6,14},{7,15},{8,0},{9,1},... | collective-permute-start | bytes 147464 | tf_op jit(solution)/shard_map/ppermute | solution.py:88
  41.7 1.3 %collective-permute-start.8 = (bf16[24,1024]{1,0:T(8,128)(2,1)S(1)}, bf16[24,1024]{1,0:T(8,128)(2,1)S(1)}, u32[]{:S(2)}, u32[]{:S(2)}) collective-permute-start(bf16[24,1024]{1,0:T(8,128)(2,1)S(1)} %fusion.7), channel_id=1, source_target_pairs={{0,1},{1,0},{2,3},{3,2},{4,5},{5,4},{6,7},{7,6},{8,9},{9,8},{10,11... | collective-permute-start | bytes 147464 | tf_op jit(solution)/shard_map/ppermute | solution.py:86

commit v4 on v3

--- a/solution.py
+++ b/solution.py
@@ -93,7 +93,14 @@
     half = width // 2
     top = routes.shape[1]
 
-    def kernel(x_ref, gain_ref, route_ref, score_ref, out_ref):
+    def kernel(*refs):
+        given, out_ref, local, sem = refs[:4], refs[4], refs[5:9], refs[9]
+        copies = [pltpu.make_async_copy(a, b, sem.at[i]) for i, (a, b) in enumerate(zip(given, local))]
+        for copy in copies:
+            copy.start()
+        for copy in copies:
+            copy.wait()
+        x_ref, gain_ref, route_ref, score_ref = local
         first = lax.axis_index("tp") == 0
         x = x_ref[...].astype(jnp.float32)
         scale = lax.rsqrt(jnp.mean(x * x, axis=-1, keepdims=True) + 1e-06)
@@ -112,12 +119,16 @@
         turned = lax.dot_general(term, unit, (((0,), (0,)), ((), ())), preferred_element_type=jnp.float32)
         out_ref[:, half:] = turned.astype(jnp.bfloat16)
 
+    args = (tokens, norm_gain[None, :], routes.T, gate_scores.T)
     return pl.pallas_call(
         kernel,
+        in_specs=[pl.BlockSpec(memory_space=pltpu.HBM)] * len(args),
         out_shape=pltpu.VMEM((count, half + lanes), jnp.bfloat16),
+        scratch_shapes=[pltpu.VMEM(a.shape, a.dtype) for a in args]
+        + [pltpu.SemaphoreType.DMA((len(args),))],
         compiler_params=pltpu.CompilerParams(vmem_limit_bytes=4 << 20),
         name="prepare",
-    )(tokens, norm_gain[None, :], routes.T, gate_scores.T)
+    )(*[pltpu.with_memory_space_constraint(a, pltpu.HBM) for a in args])
 
 
 def dense(tokens, norm_gain, routes, gate_scores, w_gate, w_up, w_down):

time: 44 us -> 41.9 us (0.952)
  local copies, waits for them, and re-layouts: 4.52 us -> 1.57 us
  Pallas kernels: 0.2 us -> 1.13 us
    unnamed x14 -> x6, local copies, waits for them, and re-layouts: 2.98 us -> 0.03 us
    pallas_call x1, Pallas kernels: 0.2 us -> 1.13 us  [prepare(): pl.pallas_call(kernel, in_specs=[pl.BlockSpec(memory_space=pltpu.HBM)] *...]
where the time goes in v4:
time: 41.9 us; the launch traced here: 41.7 us
  waiting for transfers between devices  22.9 us (55%)
  starting transfers between devices  13.4 us (32%)
  local copies, waits for them, and re-layouts  1.57 us (4%)
  matrix products  1.31 us (3%)
  other arithmetic  1.27 us (3%)
  Pallas kernels  1.13 us (3%)
    ppermute x6, waiting for transfers between devices, swap(): return lax.ppermute(x, ('ep', 'tp'), pairs)  18.8 us
    ppermute x6, starting transfers between devices, swap(): return lax.ppermute(x, ('ep', 'tp'), pairs)  13 us
    ppermute x3, waiting for transfers between devices, swap(): return lax.ppermute(x, 'tp', [(c, c ^ 1) for c in range(cores)])  4.14 us
    dynamic_slice x2, local copies, waits for them, and re-layouts, own_first(): return (own, lax.dynamic_slice_in_dim(w, (1 - tp) * half, half, axis))  1.5 us
    pallas_call x1, Pallas kernels, prepare(): pl.pallas_call(kernel, in_specs=[pl.BlockSpec(memory_space=pltpu.HBM)] *...  1.13 us
  transfers between devices with their start and end apart: 9, of which 9 were waited for; matrix products, arithmetic and copies ran while one was open for 4% of the time, Pallas kernels for 0%

profile of v4, /device:TPU:0, one launch (start us, length us, event | category | flops | bytes accessed | tf_op | source)
XLA Modules:
  0.0 41.7 jit_solution(17387940384129734147)
XLA Ops:
  0.0 1.1 %prepare.1 = bf16[24,1152]{1,0:T(8,128)(2,1)S(1)} custom-call(bf16[24,2048]{1,0:T(8,128)(2,1)} %refs_0_.1, f32[1,2048]{1,0:T(1,128)} %bitcast.21, s32[4,24]{1,0:T(4,128)} %bitcast.22, f32[4,24]{1,0:T(4,128)} %bitcast.23), custom_call_target="tpu_custom_call" | custom-call | tf_op jit(solution)/shard_map/prepare/pallas_call | solution.py:123
  1.1 4.1 %collective-permute-start = (bf16[24,1152]{1,0:T(8,128)(2,1)S(1)}, bf16[24,1152]{1,0:T(8,128)(2,1)S(1)}, u32[]{:S(2)}, u32[]{:S(2)}) collective-permute-start(bf16[24,1152]{1,0:T(8,128)(2,1)S(1)} %prepare.1), channel_id=1, source_target_pairs={{0,8},{1,9},{2,10},{3,11},{4,12},{5,13},{6,14},{7,15},{8,0},{9,1},... | collective-permute-start | bytes 165896 | tf_op jit(solution)/shard_map/ppermute | solution.py:88
  5.3 2.7 %collective-permute-done = bf16[24,1152]{1,0:T(8,128)(2,1)S(1)} collective-permute-done((bf16[24,1152]{1,0:T(8,128)(2,1)S(1)}, bf16[24,1152]{1,0:T(8,128)(2,1)S(1)}, u32[]{:S(2)}, u32[]{:S(2)}) %collective-permute-start) | collective-permute-done | bytes 55328 | tf_op jit(solution)/shard_map/ppermute | solution.py:88
  8.0 1.4 %collective-permute-start.1 = (bf16[48,1152]{1,0:T(8,128)(2,1)S(1)}, bf16[48,1152]{1,0:T(8,128)(2,1)S(1)}, u32[]{:S(2)}, u32[]{:S(2)}) collective-permute-start(bf16[48,1152]{1,0:T(8,128)(2,1)S(1)} %pad_maximum_fusion.4), channel_id=1, source_target_pairs={{0,4},{1,3},{2,6},{3,1},{4,0},{5,7},{6,2},{7,5},{8,12},{9,11},{10,... | collective-permute-start | bytes 331784 | tf_op jit(solution)/shard_map/ppermute | solution.py:88
  9.4 0.0 copy-start.1
  9.4 1.4 %dynamic-slice_bitcast_fusion = (bf16[256,1024]{1,0:T(8,128)(2,1)S(1)}, bf16[256,1024]{1,0:T(8,128)(2,1)S(1)}) fusion(bf16[1,256,2048]{2,1,0:T(8,128)(2,1)} %param.13, s32[]{:T(128)S(6)} %select_n.55, s32[]{:T(128)S(6)} %select_n.54), kind=kLoop, calls=%fused_computation.5 | loop fusion | bytes 2097160 | tf_op jit(solution)/shard_map/dynamic_slice | solution.py:149
  10.8 0.0 copy-start
  10.8 2.2 %collective-permute-done.1 = bf16[48,1152]{1,0:T(8,128)(2,1)S(1)} collective-permute-done((bf16[48,1152]{1,0:T(8,128)(2,1)S(1)}, bf16[48,1152]{1,0:T(8,128)(2,1)S(1)}, u32[]{:S(2)}, u32[]{:S(2)}) %collective-permute-start.1) | collective-permute-done | bytes 110624 | tf_op jit(solution)/shard_map/ppermute | solution.py:88
  12.9 1.9 %collective-permute-start.2 = (bf16[96,1152]{1,0:T(8,128)(2,1)S(1)}, bf16[96,1152]{1,0:T(8,128)(2,1)S(1)}, u32[]{:S(2)}, u32[]{:S(2)}) collective-permute-start(bf16[96,1152]{1,0:T(8,128)(2,1)S(1)} %pad_maximum_fusion.2), channel_id=1, source_target_pairs={{0,2},{1,5},{2,0},{3,7},{4,6},{5,1},{6,4},{7,3},{8,10},{9,13},{10,... | collective-permute-start | bytes 663560 | tf_op jit(solution)/shard_map/ppermute | solution.py:88
  14.9 4.0 %collective-permute-done.2 = bf16[96,1152]{1,0:T(8,128)(2,1)S(1)} collective-permute-done((bf16[96,1152]{1,0:T(8,128)(2,1)S(1)}, bf16[96,1152]{1,0:T(8,128)(2,1)S(1)}, u32[]{:S(2)}, u32[]{:S(2)}) %collective-permute-start.2) | collective-permute-done | bytes 221216 | tf_op jit(solution)/shard_map/ppermute | solution.py:88
  19.0 0.1 collective-permute-start.3
  19.1 0.0 copy-done.1
  19.1 0.0 copy-done
  19.1 0.1 dynamic-slice_bitcast_fusion.2
  19.3 0.1 pad_maximum_fusion
  19.4 0.1 pad_maximum_fusion.1
  19.5 1.4 %collective-permute-done.3 = bf16[192,1152]{1,0:T(8,128)(2,1)S(1)} collective-permute-done((bf16[192,1152]{1,0:T(8,128)(2,1)S(1)}, bf16[192,1152]{1,0:T(8,128)(2,1)S(1)}, u32[]{:S(2)}, u32[]{:S(2)}) %collective-permute-start.3) | collective-permute-done | bytes 442400 | tf_op jit(solution)/shard_map/ppermute | solution.py:86
  20.9 0.4 fusion
  21.3 0.4 convolution_add_fusion
  21.7 0.1 fusion.6
  21.8 0.3 convolution_convert_fusion
  22.0 0.2 collective-permute-start.4
  22.2 0.1 select_reduce_fusion
  22.4 1.5 %collective-permute-done.4 = bf16[192,1024]{1,0:T(8,128)(2,1)S(1)} collective-permute-done((bf16[192,1024]{1,0:T(8,128)(2,1)S(1)}, bf16[192,1024]{1,0:T(8,128)(2,1)S(1)}, u32[]{:S(2)}, u32[]{:S(2)}) %collective-permute-start.4) | collective-permute-done | bytes 393248 | tf_op jit(solution)/shard_map/ppermute | solution.py:86
  23.8 0.3 add_multiply_fusion
  24.2 1.9 %collective-permute-start.5 = (bf16[96,1024]{1,0:T(8,128)(2,1)S(1)}, bf16[96,1024]{1,0:T(8,128)(2,1)S(1)}, u32[]{:S(2)}, u32[]{:S(2)}) collective-permute-start(bf16[96,1024]{1,0:T(8,128)(2,1)S(1)} %pad_maximum_fusion.3), channel_id=1, source_target_pairs={{0,2},{1,5},{2,0},{3,7},{4,6},{5,1},{6,4},{7,3},{8,10},{9,13},{10,... | collective-permute-start | bytes 589832 | tf_op jit(solution)/shard_map/ppermute | solution.py:88
  26.1 3.8 %collective-permute-done.5 = bf16[96,1024]{1,0:T(8,128)(2,1)S(1)} collective-permute-done((bf16[96,1024]{1,0:T(8,128)(2,1)S(1)}, bf16[96,1024]{1,0:T(8,128)(2,1)S(1)}, u32[]{:S(2)}, u32[]{:S(2)}) %collective-permute-start.5) | collective-permute-done | bytes 196640 | tf_op jit(solution)/shard_map/ppermute | solution.py:88
  30.0 1.3 %collective-permute-start.6 = (bf16[48,1024]{1,0:T(8,128)(2,1)S(1)}, bf16[48,1024]{1,0:T(8,128)(2,1)S(1)}, u32[]{:S(2)}, u32[]{:S(2)}) collective-permute-start(bf16[48,1024]{1,0:T(8,128)(2,1)S(1)} %slice.115), channel_id=1, source_target_pairs={{0,4},{1,3},{2,6},{3,1},{4,0},{5,7},{6,2},{7,5},{8,12},{9,11},{10,... | collective-permute-start | bytes 294920 | tf_op jit(solution)/shard_map/ppermute | solution.py:88
  31.2 3.4 %collective-permute-done.6 = bf16[48,1024]{1,0:T(8,128)(2,1)S(1)} collective-permute-done((bf16[48,1024]{1,0:T(8,128)(2,1)S(1)}, bf16[48,1024]{1,0:T(8,128)(2,1)S(1)}, u32[]{:S(2)}, u32[]{:S(2)}) %collective-permute-start.6) | collective-permute-done | bytes 98336 | tf_op jit(solution)/shard_map/ppermute | solution.py:88
  34.7 2.4 %collective-permute-start.7 = (bf16[24,1024]{1,0:T(8,128)(2,1)S(1)}, bf16[24,1024]{1,0:T(8,128)(2,1)S(1)}, u32[]{:S(2)}, u32[]{:S(2)}) collective-permute-start(bf16[24,1024]{1,0:T(8,128)(2,1)S(1)} %slice.117), channel_id=1, source_target_pairs={{0,8},{1,9},{2,10},{3,11},{4,12},{5,13},{6,14},{7,15},{8,0},{9,1},... | collective-permute-start | bytes 147464 | tf_op jit(solution)/shard_map/ppermute | solution.py:88
  37.1 2.7 %collective-permute-done.7 = bf16[24,1024]{1,0:T(8,128)(2,1)S(1)} collective-permute-done((bf16[24,1024]{1,0:T(8,128)(2,1)S(1)}, bf16[24,1024]{1,0:T(8,128)(2,1)S(1)}, u32[]{:S(2)}, u32[]{:S(2)}) %collective-permute-start.7) | collective-permute-done | bytes 49184 | tf_op jit(solution)/shard_map/ppermute | solution.py:88
  39.8 0.1 collective-permute-start.8
  39.8 1.2 %collective-permute-done.8 = bf16[24,1024]{1,0:T(8,128)(2,1)S(1)} collective-permute-done((bf16[24,1024]{1,0:T(8,128)(2,1)S(1)}, bf16[24,1024]{1,0:T(8,128)(2,1)S(1)}, u32[]{:S(2)}, u32[]{:S(2)}) %collective-permute-start.8) | collective-permute-done | bytes 49184 | tf_op jit(solution)/shard_map/ppermute | solution.py:86
  41.1 0.6 %pad_maximum_fusion.5 = bf16[24,2048]{1,0:T(8,128)(2,1)} fusion(bf16[24,1024]{1,0:T(8,128)(2,1)S(1)} %get-tuple-element.24, bf16[24,1024]{1,0:T(8,128)(2,1)S(1)} %get-tuple-element.23), kind=kLoop, calls=%fused_computation.35 | loop fusion | flops 196608 | bytes 196608 | tf_op jit(solution)/shard_map/concatenate | solution.py:190
  (17 shorter events, 0.3 us)
Async XLA Ops:
  1.1 6.9 %collective-permute-start = (bf16[24,1152]{1,0:T(8,128)(2,1)S(1)}, bf16[24,1152]{1,0:T(8,128)(2,1)S(1)}, u32[]{:S(2)}, u32[]{:S(2)}) collective-permute-start(bf16[24,1152]{1,0:T(8,128)(2,1)S(1)} %prepare.1), channel_id=1, source_target_pairs={{0,8},{1,9},{2,10},{3,11},{4,12},{5,13},{6,14},{7,15},{8,0},{9,1},... | collective-permute-start | bytes 165896 | tf_op jit(solution)/shard_map/ppermute | solution.py:88
  8.0 4.9 %collective-permute-start.1 = (bf16[48,1152]{1,0:T(8,128)(2,1)S(1)}, bf16[48,1152]{1,0:T(8,128)(2,1)S(1)}, u32[]{:S(2)}, u32[]{:S(2)}) collective-permute-start(bf16[48,1152]{1,0:T(8,128)(2,1)S(1)} %pad_maximum_fusion.4), channel_id=1, source_target_pairs={{0,4},{1,3},{2,6},{3,1},{4,0},{5,7},{6,2},{7,5},{8,12},{9,11},{10,... | collective-permute-start | bytes 331784 | tf_op jit(solution)/shard_map/ppermute | solution.py:88
  9.4 9.7 %copy-start.1 = (bf16[1,2048,256]{2,1,0:T(8,128)(2,1)S(1)}, bf16[1,2048,256]{2,1,0:T(8,128)(2,1)}, u32[]{:S(2)}) copy-start(bf16[1,2048,256]{2,1,0:T(8,128)(2,1)} %param.11) | copy-start | bytes 3145732
  10.8 8.4 %copy-start = (bf16[1,2048,256]{2,1,0:T(8,128)(2,1)S(1)}, bf16[1,2048,256]{2,1,0:T(8,128)(2,1)}, u32[]{:S(2)}) copy-start(bf16[1,2048,256]{2,1,0:T(8,128)(2,1)} %param.12) | copy-start | bytes 3145732
  12.9 6.0 %collective-permute-start.2 = (bf16[96,1152]{1,0:T(8,128)(2,1)S(1)}, bf16[96,1152]{1,0:T(8,128)(2,1)S(1)}, u32[]{:S(2)}, u32[]{:S(2)}) collective-permute-start(bf16[96,1152]{1,0:T(8,128)(2,1)S(1)} %pad_maximum_fusion.2), channel_id=1, source_target_pairs={{0,2},{1,5},{2,0},{3,7},{4,6},{5,1},{6,4},{7,3},{8,10},{9,13},{10,... | collective-permute-start | bytes 663560 | tf_op jit(solution)/shard_map/ppermute | solution.py:88
  19.0 1.9 %collective-permute-start.3 = (bf16[192,1152]{1,0:T(8,128)(2,1)S(1)}, bf16[192,1152]{1,0:T(8,128)(2,1)S(1)}, u32[]{:S(2)}, u32[]{:S(2)}) collective-permute-start(bf16[192,1152]{1,0:T(8,128)(2,1)S(1)} %slice_dynamic-update-slice_fusion), channel_id=1, source_target_pairs={{0,1},{1,0},{2,3},{3,2},{4,5},{5,4},{6,7},{7,6},{8,9},{9,8},{10,11... | collective-permute-start | bytes 1327112 | tf_op jit(solution)/shard_map/ppermute | solution.py:86
  22.0 1.8 %collective-permute-start.4 = (bf16[192,1024]{1,0:T(8,128)(2,1)S(1)}, bf16[192,1024]{1,0:T(8,128)(2,1)S(1)}, u32[]{:S(2)}, u32[]{:S(2)}) collective-permute-start(bf16[192,1024]{1,0:T(8,128)(2,1)S(1)} %convolution_convert_fusion), channel_id=1, source_target_pairs={{0,1},{1,0},{2,3},{3,2},{4,5},{5,4},{6,7},{7,6},{8,9},{9,8},{10,11... | collective-permute-start | bytes 1179656 | tf_op jit(solution)/shard_map/ppermute | solution.py:86
  24.2 5.7 %collective-permute-start.5 = (bf16[96,1024]{1,0:T(8,128)(2,1)S(1)}, bf16[96,1024]{1,0:T(8,128)(2,1)S(1)}, u32[]{:S(2)}, u32[]{:S(2)}) collective-permute-start(bf16[96,1024]{1,0:T(8,128)(2,1)S(1)} %pad_maximum_fusion.3), channel_id=1, source_target_pairs={{0,2},{1,5},{2,0},{3,7},{4,6},{5,1},{6,4},{7,3},{8,10},{9,13},{10,... | collective-permute-start | bytes 589832 | tf_op jit(solution)/shard_map/ppermute | solution.py:88
  30.0 4.7 %collective-permute-start.6 = (bf16[48,1024]{1,0:T(8,128)(2,1)S(1)}, bf16[48,1024]{1,0:T(8,128)(2,1)S(1)}, u32[]{:S(2)}, u32[]{:S(2)}) collective-permute-start(bf16[48,1024]{1,0:T(8,128)(2,1)S(1)} %slice.115), channel_id=1, source_target_pairs={{0,4},{1,3},{2,6},{3,1},{4,0},{5,7},{6,2},{7,5},{8,12},{9,11},{10,... | collective-permute-start | bytes 294920 | tf_op jit(solution)/shard_map/ppermute | solution.py:88
  34.7 5.1 %collective-permute-start.7 = (bf16[24,1024]{1,0:T(8,128)(2,1)S(1)}, bf16[24,1024]{1,0:T(8,128)(2,1)S(1)}, u32[]{:S(2)}, u32[]{:S(2)}) collective-permute-start(bf16[24,1024]{1,0:T(8,128)(2,1)S(1)} %slice.117), channel_id=1, source_target_pairs={{0,8},{1,9},{2,10},{3,11},{4,12},{5,13},{6,14},{7,15},{8,0},{9,1},... | collective-permute-start | bytes 147464 | tf_op jit(solution)/shard_map/ppermute | solution.py:88
  39.8 1.3 %collective-permute-start.8 = (bf16[24,1024]{1,0:T(8,128)(2,1)S(1)}, bf16[24,1024]{1,0:T(8,128)(2,1)S(1)}, u32[]{:S(2)}, u32[]{:S(2)}) collective-permute-start(bf16[24,1024]{1,0:T(8,128)(2,1)S(1)} %fusion.7), channel_id=1, source_target_pairs={{0,1},{1,0},{2,3},{3,2},{4,5},{5,4},{6,7},{7,6},{8,9},{9,8},{10,11... | collective-permute-start | bytes 147464 | tf_op jit(solution)/shard_map/ppermute | solution.py:86

commit v5 on v4

--- a/solution.py
+++ b/solution.py
@@ -166,8 +166,8 @@
         [rows[:n], jnp.where(first, one, two), jnp.where(first, two, one), far[n:]], axis=0
     )
     other = swap(own, None)
-    h = jnp.dot(own[:, :half], in_own, preferred_element_type=jnp.float32)
-    h = h + jnp.dot(other[:, :half], in_other, preferred_element_type=jnp.float32)
+    h = jnp.dot(other[:, :half], in_other, preferred_element_type=jnp.float32)
+    h = h + jnp.dot(own[:, :half], in_own, preferred_element_type=jnp.float32)
     pair = own[:, half:].astype(jnp.float32) + other[:, half:].astype(jnp.float32)
     mine = (jnp.arange(lanes, dtype=jnp.int32) == lax.axis_index("ep"))[None, :]
     score = jnp.sum(jnp.where(mine, pair, 0.0), axis=1, keepdims=True)

time: 41.9 us -> 41.9 us (level)
  waiting for transfers between devices: 22.9 us -> 20 us
  local copies, waits for them, and re-layouts: 1.57 us -> 3.36 us
  other arithmetic: 1.27 us -> 2.07 us
    ppermute x6, waiting for transfers between devices: 18.8 us -> 16.9 us  [swap(): return lax.ppermute(x, ('ep', 'tp'), pairs)]
    dynamic_slice x2, local copies, waits for them, and re-layouts: 1.5 us -> 2.92 us  [own_first(): return (own, lax.dynamic_slice_in_dim(w, (1 - tp) * half, half, axis))]
    ppermute x3, waiting for transfers between devices: 4.14 us -> 3.1 us  [swap(): return lax.ppermute(x, 'tp', [(c, c ^ 1) for c in range(cores)])]
    reduce_sum x1, other arithmetic: 0.12 us -> 0.91 us  [dense(): score = jnp.sum(jnp.where(mine, pair, 0.0), axis=1, keepdims=True)]
  transfers between devices with their start and end apart: 9 -> 9, of which waited for: 9 -> 9; matrix products, arithmetic and copies ran while one was open for 4% -> 11% of each run, Pallas kernels for 0% -> 0%
where the time goes in v5:
time: 41.9 us; the launch traced here: 41.6 us
  waiting for transfers between devices  20 us (48%)
  starting transfers between devices  13.6 us (32%)
  local copies, waits for them, and re-layouts  3.36 us (8%)
  other arithmetic  2.07 us (5%)
  matrix products  1.29 us (3%)
  Pallas kernels  1.13 us (3%)
    ppermute x6, waiting for transfers between devices, swap(): return lax.ppermute(x, ('ep', 'tp'), pairs)  16.9 us
    ppermute x6, starting transfers between devices, swap(): return lax.ppermute(x, ('ep', 'tp'), pairs)  13.3 us
    ppermute x3, waiting for transfers between devices, swap(): return lax.ppermute(x, 'tp', [(c, c ^ 1) for c in range(cores)])  3.1 us
    dynamic_slice x2, local copies, waits for them, and re-layouts, own_first(): return (own, lax.dynamic_slice_in_dim(w, (1 - tp) * half, half, axis))  2.92 us
    pallas_call x1, Pallas kernels, prepare(): pl.pallas_call(kernel, in_specs=[pl.BlockSpec(memory_space=pltpu.HBM)] *...  1.13 us
    reduce_sum x1, other arithmetic, dense(): score = jnp.sum(jnp.where(mine, pair, 0.0), axis=1, keepdims=True)  0.91 us
  transfers between devices with their start and end apart: 9, of which 9 were waited for; matrix products, arithmetic and copies ran while one was open for 11% of the time, Pallas kernels for 0%

profile of v5, /device:TPU:0, one launch (start us, length us, event | category | flops | bytes accessed | tf_op | source)
XLA Modules:
  0.0 41.6 jit_solution(7878214284062092533)
XLA Ops:
  0.0 1.1 %prepare.1 = bf16[24,1152]{1,0:T(8,128)(2,1)S(1)} custom-call(bf16[24,2048]{1,0:T(8,128)(2,1)} %refs_0_.1, f32[1,2048]{1,0:T(1,128)} %bitcast.21, s32[4,24]{1,0:T(4,128)} %bitcast.22, f32[4,24]{1,0:T(4,128)} %bitcast.23), custom_call_target="tpu_custom_call" | custom-call | tf_op jit(solution)/shard_map/prepare/pallas_call | solution.py:123
  1.1 4.1 %collective-permute-start = (bf16[24,1152]{1,0:T(8,128)(2,1)S(1)}, bf16[24,1152]{1,0:T(8,128)(2,1)S(1)}, u32[]{:S(2)}, u32[]{:S(2)}) collective-permute-start(bf16[24,1152]{1,0:T(8,128)(2,1)S(1)} %prepare.1), channel_id=1, source_target_pairs={{0,8},{1,9},{2,10},{3,11},{4,12},{5,13},{6,14},{7,15},{8,0},{9,1},... | collective-permute-start | bytes 165896 | tf_op jit(solution)/shard_map/ppermute | solution.py:88
  5.3 1.7 %dynamic-slice_bitcast_fusion.2 = (bf16[1024,256]{1,0:T(8,128)(2,1)S(1)}, bf16[1024,256]{1,0:T(8,128)(2,1)S(1)}, bf16[1024,256]{1,0:T(8,128)(2,1)S(1)}, bf16[1024,256]{1,0:T(8,128)(2,1)S(1)}) fusion(bf16[1,2048,256]{2,1,0:T(8,128)(2,1)} %param.12, s32[]{:T(128)S(6)} %select_n.55, s32[]{:T(128)S(6)} %select_n.54, bf16[1,2048,256]{2,1,0:T(8,128)(2,1)} %param.11), kind=kLoop, calls=%fused_computation.7 | loop fusion | bytes 4194312 | tf_op jit(solution)/shard_map/dynamic_slice | solution.py:149
  6.9 1.1 %collective-permute-done = bf16[24,1152]{1,0:T(8,128)(2,1)S(1)} collective-permute-done((bf16[24,1152]{1,0:T(8,128)(2,1)S(1)}, bf16[24,1152]{1,0:T(8,128)(2,1)S(1)}, u32[]{:S(2)}, u32[]{:S(2)}) %collective-permute-start) | collective-permute-done | bytes 55328 | tf_op jit(solution)/shard_map/ppermute | solution.py:88
  8.0 1.4 %collective-permute-start.1 = (bf16[48,1152]{1,0:T(8,128)(2,1)S(1)}, bf16[48,1152]{1,0:T(8,128)(2,1)S(1)}, u32[]{:S(2)}, u32[]{:S(2)}) collective-permute-start(bf16[48,1152]{1,0:T(8,128)(2,1)S(1)} %pad_maximum_fusion.4), channel_id=1, source_target_pairs={{0,4},{1,3},{2,6},{3,1},{4,0},{5,7},{6,2},{7,5},{8,12},{9,11},{10,... | collective-permute-start | bytes 331784 | tf_op jit(solution)/shard_map/ppermute | solution.py:88
  9.4 1.3 %dynamic-slice_bitcast_fusion = (bf16[256,1024]{1,0:T(8,128)(2,1)S(1)}, bf16[256,1024]{1,0:T(8,128)(2,1)S(1)}) fusion(bf16[1,256,2048]{2,1,0:T(8,128)(2,1)} %param.13, s32[]{:T(128)S(6)} %select_n.55, s32[]{:T(128)S(6)} %select_n.54), kind=kLoop, calls=%fused_computation.5 | loop fusion | bytes 2097160 | tf_op jit(solution)/shard_map/dynamic_slice | solution.py:149
  10.7 2.2 %collective-permute-done.1 = bf16[48,1152]{1,0:T(8,128)(2,1)S(1)} collective-permute-done((bf16[48,1152]{1,0:T(8,128)(2,1)S(1)}, bf16[48,1152]{1,0:T(8,128)(2,1)S(1)}, u32[]{:S(2)}, u32[]{:S(2)}) %collective-permute-start.1) | collective-permute-done | bytes 110624 | tf_op jit(solution)/shard_map/ppermute | solution.py:88
  12.8 2.0 %collective-permute-start.2 = (bf16[96,1152]{1,0:T(8,128)(2,1)S(1)}, bf16[96,1152]{1,0:T(8,128)(2,1)S(1)}, u32[]{:S(2)}, u32[]{:S(2)}) collective-permute-start(bf16[96,1152]{1,0:T(8,128)(2,1)S(1)} %pad_maximum_fusion.2), channel_id=1, source_target_pairs={{0,2},{1,5},{2,0},{3,7},{4,6},{5,1},{6,4},{7,3},{8,10},{9,13},{10,... | collective-permute-start | bytes 663560 | tf_op jit(solution)/shard_map/ppermute | solution.py:88
  14.8 4.0 %collective-permute-done.2 = bf16[96,1152]{1,0:T(8,128)(2,1)S(1)} collective-permute-done((bf16[96,1152]{1,0:T(8,128)(2,1)S(1)}, bf16[96,1152]{1,0:T(8,128)(2,1)S(1)}, u32[]{:S(2)}, u32[]{:S(2)}) %collective-permute-start.2) | collective-permute-done | bytes 221216 | tf_op jit(solution)/shard_map/ppermute | solution.py:88
  18.9 0.1 collective-permute-start.3
  19.0 0.1 pad_maximum_fusion
  19.1 0.1 pad_maximum_fusion.1
  19.2 0.4 fusion
  19.6 1.2 %collective-permute-done.3 = bf16[192,1152]{1,0:T(8,128)(2,1)S(1)} collective-permute-done((bf16[192,1152]{1,0:T(8,128)(2,1)S(1)}, bf16[192,1152]{1,0:T(8,128)(2,1)S(1)}, u32[]{:S(2)}, u32[]{:S(2)}) %collective-permute-start.3) | collective-permute-done | bytes 442400 | tf_op jit(solution)/shard_map/ppermute | solution.py:86
  20.8 0.0 copy-start
  20.8 0.4 convolution_add_fusion
  21.2 0.4 copy-done
  21.6 0.1 fusion.6
  21.7 0.3 convolution_convert_fusion
  21.9 0.2 collective-permute-start.4
  22.1 0.9 %select_reduce_fusion = f32[192]{0:T(256)S(1)} fusion(bf16[192,1152]{1,0:T(8,128)(2,1)} %copy-done, bf16[192,1152]{1,0:T(8,128)(2,1)S(1)} %slice_dynamic-update-slice_fusion, pred[128]{0:T(512)(128)(4,1)S(1)} %iota_compare_fusion), kind=kLoop, calls=%fused_computation.36 | loop fusion | flops 122688 | bytes 99200 | tf_op jit(solution)/shard_map/reduce_sum | solution.py:173
  23.1 0.7 %collective-permute-done.4 = bf16[192,1024]{1,0:T(8,128)(2,1)S(1)} collective-permute-done((bf16[192,1024]{1,0:T(8,128)(2,1)S(1)}, bf16[192,1024]{1,0:T(8,128)(2,1)S(1)}, u32[]{:S(2)}, u32[]{:S(2)}) %collective-permute-start.4) | collective-permute-done | bytes 393248 | tf_op jit(solution)/shard_map/ppermute | solution.py:86
  23.7 0.3 add_multiply_fusion
  24.1 1.9 %collective-permute-start.5 = (bf16[96,1024]{1,0:T(8,128)(2,1)S(1)}, bf16[96,1024]{1,0:T(8,128)(2,1)S(1)}, u32[]{:S(2)}, u32[]{:S(2)}) collective-permute-start(bf16[96,1024]{1,0:T(8,128)(2,1)S(1)} %pad_maximum_fusion.3), channel_id=1, source_target_pairs={{0,2},{1,5},{2,0},{3,7},{4,6},{5,1},{6,4},{7,3},{8,10},{9,13},{10,... | collective-permute-start | bytes 589832 | tf_op jit(solution)/shard_map/ppermute | solution.py:88
  26.1 3.7 %collective-permute-done.5 = bf16[96,1024]{1,0:T(8,128)(2,1)S(1)} collective-permute-done((bf16[96,1024]{1,0:T(8,128)(2,1)S(1)}, bf16[96,1024]{1,0:T(8,128)(2,1)S(1)}, u32[]{:S(2)}, u32[]{:S(2)}) %collective-permute-start.5) | collective-permute-done | bytes 196640 | tf_op jit(solution)/shard_map/ppermute | solution.py:88
  29.9 1.4 %collective-permute-start.6 = (bf16[48,1024]{1,0:T(8,128)(2,1)S(1)}, bf16[48,1024]{1,0:T(8,128)(2,1)S(1)}, u32[]{:S(2)}, u32[]{:S(2)}) collective-permute-start(bf16[48,1024]{1,0:T(8,128)(2,1)S(1)} %slice.115), channel_id=1, source_target_pairs={{0,4},{1,3},{2,6},{3,1},{4,0},{5,7},{6,2},{7,5},{8,12},{9,11},{10,... | collective-permute-start | bytes 294920 | tf_op jit(solution)/shard_map/ppermute | solution.py:88
  31.2 3.3 %collective-permute-done.6 = bf16[48,1024]{1,0:T(8,128)(2,1)S(1)} collective-permute-done((bf16[48,1024]{1,0:T(8,128)(2,1)S(1)}, bf16[48,1024]{1,0:T(8,128)(2,1)S(1)}, u32[]{:S(2)}, u32[]{:S(2)}) %collective-permute-start.6) | collective-permute-done | bytes 98336 | tf_op jit(solution)/shard_map/ppermute | solution.py:88
  34.6 2.5 %collective-permute-start.7 = (bf16[24,1024]{1,0:T(8,128)(2,1)S(1)}, bf16[24,1024]{1,0:T(8,128)(2,1)S(1)}, u32[]{:S(2)}, u32[]{:S(2)}) collective-permute-start(bf16[24,1024]{1,0:T(8,128)(2,1)S(1)} %slice.117), channel_id=1, source_target_pairs={{0,8},{1,9},{2,10},{3,11},{4,12},{5,13},{6,14},{7,15},{8,0},{9,1},... | collective-permute-start | bytes 147464 | tf_op jit(solution)/shard_map/ppermute | solution.py:88
  37.1 2.6 %collective-permute-done.7 = bf16[24,1024]{1,0:T(8,128)(2,1)S(1)} collective-permute-done((bf16[24,1024]{1,0:T(8,128)(2,1)S(1)}, bf16[24,1024]{1,0:T(8,128)(2,1)S(1)}, u32[]{:S(2)}, u32[]{:S(2)}) %collective-permute-start.7) | collective-permute-done | bytes 49184 | tf_op jit(solution)/shard_map/ppermute | solution.py:88
  39.7 0.1 collective-permute-start.8
  39.7 1.2 %collective-permute-done.8 = bf16[24,1024]{1,0:T(8,128)(2,1)S(1)} collective-permute-done((bf16[24,1024]{1,0:T(8,128)(2,1)S(1)}, bf16[24,1024]{1,0:T(8,128)(2,1)S(1)}, u32[]{:S(2)}, u32[]{:S(2)}) %collective-permute-start.8) | collective-permute-done | bytes 49184 | tf_op jit(solution)/shard_map/ppermute | solution.py:86
  41.0 0.6 %pad_maximum_fusion.5 = bf16[24,2048]{1,0:T(8,128)(2,1)} fusion(bf16[24,1024]{1,0:T(8,128)(2,1)S(1)} %get-tuple-element.24, bf16[24,1024]{1,0:T(8,128)(2,1)S(1)} %get-tuple-element.23), kind=kLoop, calls=%fused_computation.35 | loop fusion | flops 196608 | bytes 196608 | tf_op jit(solution)/shard_map/concatenate | solution.py:190
  (17 shorter events, 0.3 us)
Async XLA Ops:
  1.1 6.9 %collective-permute-start = (bf16[24,1152]{1,0:T(8,128)(2,1)S(1)}, bf16[24,1152]{1,0:T(8,128)(2,1)S(1)}, u32[]{:S(2)}, u32[]{:S(2)}) collective-permute-start(bf16[24,1152]{1,0:T(8,128)(2,1)S(1)} %prepare.1), channel_id=1, source_target_pairs={{0,8},{1,9},{2,10},{3,11},{4,12},{5,13},{6,14},{7,15},{8,0},{9,1},... | collective-permute-start | bytes 165896 | tf_op jit(solution)/shard_map/ppermute | solution.py:88
  8.0 4.8 %collective-permute-start.1 = (bf16[48,1152]{1,0:T(8,128)(2,1)S(1)}, bf16[48,1152]{1,0:T(8,128)(2,1)S(1)}, u32[]{:S(2)}, u32[]{:S(2)}) collective-permute-start(bf16[48,1152]{1,0:T(8,128)(2,1)S(1)} %pad_maximum_fusion.4), channel_id=1, source_target_pairs={{0,4},{1,3},{2,6},{3,1},{4,0},{5,7},{6,2},{7,5},{8,12},{9,11},{10,... | collective-permute-start | bytes 331784 | tf_op jit(solution)/shard_map/ppermute | solution.py:88
  12.8 6.0 %collective-permute-start.2 = (bf16[96,1152]{1,0:T(8,128)(2,1)S(1)}, bf16[96,1152]{1,0:T(8,128)(2,1)S(1)}, u32[]{:S(2)}, u32[]{:S(2)}) collective-permute-start(bf16[96,1152]{1,0:T(8,128)(2,1)S(1)} %pad_maximum_fusion.2), channel_id=1, source_target_pairs={{0,2},{1,5},{2,0},{3,7},{4,6},{5,1},{6,4},{7,3},{8,10},{9,13},{10,... | collective-permute-start | bytes 663560 | tf_op jit(solution)/shard_map/ppermute | solution.py:88
  18.9 1.9 %collective-permute-start.3 = (bf16[192,1152]{1,0:T(8,128)(2,1)S(1)}, bf16[192,1152]{1,0:T(8,128)(2,1)S(1)}, u32[]{:S(2)}, u32[]{:S(2)}) collective-permute-start(bf16[192,1152]{1,0:T(8,128)(2,1)S(1)} %slice_dynamic-update-slice_fusion), channel_id=1, source_target_pairs={{0,1},{1,0},{2,3},{3,2},{4,5},{5,4},{6,7},{7,6},{8,9},{9,8},{10,11... | collective-permute-start | bytes 1327112 | tf_op jit(solution)/shard_map/ppermute | solution.py:86
  20.8 0.8 %copy-start = (bf16[192,1152]{1,0:T(8,128)(2,1)}, bf16[192,1152]{1,0:T(8,128)(2,1)S(1)}, u32[]{:S(2)}) copy-start(bf16[192,1152]{1,0:T(8,128)(2,1)S(1)} %collective-permute-done.3) | copy-start | bytes 1327108
  21.9 1.8 %collective-permute-start.4 = (bf16[192,1024]{1,0:T(8,128)(2,1)S(1)}, bf16[192,1024]{1,0:T(8,128)(2,1)S(1)}, u32[]{:S(2)}, u32[]{:S(2)}) collective-permute-start(bf16[192,1024]{1,0:T(8,128)(2,1)S(1)} %convolution_convert_fusion), channel_id=1, source_target_pairs={{0,1},{1,0},{2,3},{3,2},{4,5},{5,4},{6,7},{7,6},{8,9},{9,8},{10,11... | collective-permute-start | bytes 1179656 | tf_op jit(solution)/shard_map/ppermute | solution.py:86
  24.1 5.7 %collective-permute-start.5 = (bf16[96,1024]{1,0:T(8,128)(2,1)S(1)}, bf16[96,1024]{1,0:T(8,128)(2,1)S(1)}, u32[]{:S(2)}, u32[]{:S(2)}) collective-permute-start(bf16[96,1024]{1,0:T(8,128)(2,1)S(1)} %pad_maximum_fusion.3), channel_id=1, source_target_pairs={{0,2},{1,5},{2,0},{3,7},{4,6},{5,1},{6,4},{7,3},{8,10},{9,13},{10,... | collective-permute-start | bytes 589832 | tf_op jit(solution)/shard_map/ppermute | solution.py:88
  29.9 4.7 %collective-permute-start.6 = (bf16[48,1024]{1,0:T(8,128)(2,1)S(1)}, bf16[48,1024]{1,0:T(8,128)(2,1)S(1)}, u32[]{:S(2)}, u32[]{:S(2)}) collective-permute-start(bf16[48,1024]{1,0:T(8,128)(2,1)S(1)} %slice.115), channel_id=1, source_target_pairs={{0,4},{1,3},{2,6},{3,1},{4,0},{5,7},{6,2},{7,5},{8,12},{9,11},{10,... | collective-permute-start | bytes 294920 | tf_op jit(solution)/shard_map/ppermute | solution.py:88
  34.6 5.1 %collective-permute-start.7 = (bf16[24,1024]{1,0:T(8,128)(2,1)S(1)}, bf16[24,1024]{1,0:T(8,128)(2,1)S(1)}, u32[]{:S(2)}, u32[]{:S(2)}) collective-permute-start(bf16[24,1024]{1,0:T(8,128)(2,1)S(1)} %slice.117), channel_id=1, source_target_pairs={{0,8},{1,9},{2,10},{3,11},{4,12},{5,13},{6,14},{7,15},{8,0},{9,1},... | collective-permute-start | bytes 147464 | tf_op jit(solution)/shard_map/ppermute | solution.py:88
  39.7 1.3 %collective-permute-start.8 = (bf16[24,1024]{1,0:T(8,128)(2,1)S(1)}, bf16[24,1024]{1,0:T(8,128)(2,1)S(1)}, u32[]{:S(2)}, u32[]{:S(2)}) collective-permute-start(bf16[24,1024]{1,0:T(8,128)(2,1)S(1)} %fusion.7), channel_id=1, source_target_pairs={{0,1},{1,0},{2,3},{3,2},{4,5},{5,4},{6,7},{7,6},{8,9},{9,8},{10,11... | collective-permute-start | bytes 147464 | tf_op jit(solution)/shard_map/ppermute | solution.py:86
